TPU v7x, 256 devices: a whole 4x4x8 slice. The times are simulated.
256 devices in a mesh: sp: 128 (over z, y, x), tp: 2 (over core).
Axes of the slice: x: 4, y: 4, z: 8, core: 2. Of those that a mesh axis runs over, the one named last changes fastest.
Arguments:
- queries: bfloat16 [3, 32768, 2048], P(None, 'sp', 'tp'), may hold values from -6 to 6
- keys: bfloat16 [3, 32768, 2048], P(None, 'sp', 'tp'), may hold values from -6 to 6
- values: bfloat16 [3, 32768, 2048], P(None, 'sp', 'tp'), may hold values from -6 to 6
- w_out: bfloat16 [2048, 2048], P(None, 'tp'), may hold values from -1 to 1
Outputs:
- mixed: bfloat16 [32768, 2048], P('sp', 'tp')
All inputs are finite; a program needn't handle non-finite values.
Results may differ from a plain program's by a relative error of at most 0.01.
Values may be sent and summed in bfloat16 or wider, within the bound.
No kernel may reach another device: no remote copies, remote signals or barrier semaphores. Data moves between devices by JAX's collectives and lax.ppermute only.
A program may use at most 128 MiB of HBM per device.

v0:
```python
import functools

import jax
import jax.numpy as jnp
from jax import lax
from jax.experimental import pallas as pl
from jax.experimental.pallas import tpu as pltpu
from jax.sharding import PartitionSpec as P


HEAD = 128
WINDOW = 128
ROPE_BASE = 10000.0
MASKED = -1e30
SCALE = HEAD ** (-0.5)

TOKENS = 256
LOCAL = 8
PLANE = 16
HALF = TOKENS // 2
STRIDES = {1: 4, 2: 16}
RETURN_ROWS = HALF + 16


f32 = jnp.float32
bf16 = jnp.bfloat16


def iota(shape, dim):
    return lax.broadcasted_iota(jnp.int32, shape, dim)


def turned(x, cosine, sine):
    x = x.astype(f32)
    return x * cosine + pltpu.roll(x, HEAD // 2, 1) * sine


def full_tables(cos_ref, sin_ref):
    cosine, sine = cos_ref[...], sin_ref[...]
    return jnp.concatenate([cosine, cosine], axis=1), jnp.concatenate([-sine, sine], axis=1)


def sorting(stride):
    row = iota((TOKENS, TOKENS), 0)
    token = iota((TOKENS, TOKENS), 1)
    steps = TOKENS // stride
    parity = row // HALF
    within = row % HALF
    picked = parity + 2 * (within // steps) + stride * (within % steps)
    return jnp.where(picked == token, 1.0, 0.0).astype(bf16)


def prepare_kernel(kinds, *refs):
    cos_ref, sin_ref = refs[:2]
    ins, out_ref, sort_ref, full_ref = refs[2:-3], refs[-3], refs[-2], refs[-1]

    @pl.when(pl.program_id(0) == 0)
    def _():
        for g in (1, 2):
            sort_ref[g - 1] = sorting(STRIDES[g])
        full_ref[0], full_ref[1] = full_tables(cos_ref, sin_ref)

    cosine, sine = full_ref[0], full_ref[1]
    for a, (group, kind) in enumerate(kinds):
        x = ins[a][...]
        if kind != "v":
            heads = [turned(x[:, h * HEAD : (h + 1) * HEAD], cosine, sine) for h in range(2)]
            if kind == "q":
                heads = [x * SCALE for x in heads]
            x = jnp.concatenate([x.astype(bf16) for x in heads], axis=1)
        y = jnp.dot(sort_ref[group - 1], x, preferred_element_type=f32).astype(bf16)
        for h in range(2):
            for p in range(2):
                out_ref[2 * h + p, a] = y[p * HALF : (p + 1) * HALF, h * HEAD : (h + 1) * HEAD]


def prepare(kinds, arrays, cosine, sine):
    n = len(kinds)
    table = pl.BlockSpec((TOKENS, HEAD // 2), lambda g: (0, 0))
    return pl.pallas_call(
        functools.partial(prepare_kernel, kinds),
        grid=(LOCAL // 2,),
        in_specs=[table, table]
        + [
            pl.BlockSpec((None, TOKENS, 2 * HEAD), functools.partial(lambda gr, g: (gr, 0, g), group))
            for group, _ in kinds
        ],
        out_specs=pl.BlockSpec((4, n, HALF, HEAD), lambda g: (g, 0, 0, 0)),
        out_shape=jax.ShapeDtypeStruct((PLANE, n, HALF, HEAD), bf16),
        scratch_shapes=[pltpu.VMEM((2, TOKENS, TOKENS), bf16), pltpu.VMEM((2, TOKENS, HEAD), f32)],
        cost_estimate=pl.CostEstimate(
            flops=n * LOCAL * 2 * TOKENS * TOKENS * HEAD * 4, bytes_accessed=n * 2**20, transcendentals=0
        ),
    )(cosine, sine, *arrays)


def dot_t(a, b):
    return lax.dot_general(a, b, (((1,), (1,)), ((), ())), preferred_element_type=f32)


def attend(q, k_prev, k_cur, v_prev, v_cur, prev_bias):
    row = iota((WINDOW, WINDOW), 0)
    col = iota((WINDOW, WINDOW), 1)
    s_prev = jnp.where(col >= row, dot_t(q, k_prev), MASKED)
    if prev_bias is not None:
        s_prev = jnp.minimum(s_prev, prev_bias)
    s_cur = jnp.where(col <= row, dot_t(q, k_cur), MASKED)
    row_max = jnp.max(jnp.maximum(s_prev, s_cur), axis=1, keepdims=True)
    p_prev = jnp.exp(s_prev - row_max)
    p_cur = jnp.exp(s_cur - row_max)
    row_sum = jnp.sum(p_prev + p_cur, axis=1, keepdims=True)
    total = jnp.dot(p_prev.astype(bf16), v_prev, preferred_element_type=f32)
    total += jnp.dot(p_cur.astype(bf16), v_cur, preferred_element_type=f32)
    return total / row_sum, row_max + jnp.log(row_sum)


def wide(column):
    return jnp.broadcast_to(column, (column.shape[0], HEAD))


def plane_kernel(z_ref, kv_ref, q_ref, halo_ref, out_ref, far1, log1, far2, log2):
    first = z_ref[0] == 0
    big = -MASKED

    def block1(b, carry):
        bias = jnp.where(first & (b == 0), MASKED, big)
        for r in range(2):
            rows = pl.ds(r * 64, 64)
            now = [2 * b, 2 * b + 1]
            q = jnp.concatenate([q_ref[s, 0, rows, :] for s in now], axis=0)
            cur = [jnp.concatenate([kv_ref[s, a, rows, :] for s in now], axis=0) for a in (0, 1)]
            before = [jnp.maximum(2 * b - 2, 0), jnp.maximum(2 * b - 1, 0)]
            prev = []
            for a in (0, 1):
                held = jnp.concatenate([kv_ref[s, a, rows, :] for s in before], axis=0)
                other = jnp.concatenate([halo_ref[16 + 2 * i + a, rows, :] for i in range(2)], axis=0)
                prev.append(jnp.where(b == 0, other, held))
            result, logs = attend(q, prev[0], cur[0], prev[1], cur[1], bias)
            logs = wide(logs)
            for i in range(2):
                part = slice(i * 64, (i + 1) * 64)
                target = pl.ds(r, 64, stride=2)
                far1[now[i], target, :] = result[part]
                log1[now[i], target, :] = logs[part]
        return carry

    lax.fori_loop(0, 8, block1, 0)

    def block2(r, carry):
        rows = pl.ds(pl.multiple_of(r * 16, 16), 16)
        ks = [jnp.concatenate([halo_ref[2 * i, rows, :] for i in range(8)], axis=0)]
        vs = [jnp.concatenate([halo_ref[2 * i + 1, rows, :] for i in range(8)], axis=0)]
        for b in range(2):
            ks.append(jnp.concatenate([kv_ref[8 * b + i, 2, rows, :] for i in range(8)], axis=0))
            vs.append(jnp.concatenate([kv_ref[8 * b + i, 3, rows, :] for i in range(8)], axis=0))
            q = jnp.concatenate([q_ref[8 * b + i, 1, rows, :] for i in range(8)], axis=0)
            bias = jnp.where(first, MASKED, big) if b == 0 else None
            result, logs = attend(q, ks[b], ks[b + 1], vs[b], vs[b + 1], bias)
            logs = wide(logs)
            for i in range(8):
                part = slice(i * 16, (i + 1) * 16)
                target = pl.ds(r, 16, stride=8)
                far2[8 * b + i, target, :] = result[part]
                log2[8 * b + i, target, :] = logs[part]
        return carry

    lax.fori_loop(0, 8, block2, 0)

    eye = iota((HALF, HEAD), 0) == iota((HALF, HEAD), 1)
    ones = jnp.ones((16, HALF), bf16)
    sub = iota((16, HEAD), 0)

    def merge(s, carry):
        l1, l2 = log1[s], log2[s]
        m = jnp.maximum(l1, l2)
        w1, w2 = jnp.exp(l1 - m), jnp.exp(l2 - m)
        denominator = w1 + w2
        out_ref[s, :HALF, :] = ((w1 * far1[s] + w2 * far2[s]) / denominator).astype(bf16)
        log_sum = m + jnp.log(denominator)
        high = log_sum.astype(bf16)
        low = (log_sum - high.astype(f32)).astype(bf16)
        zero = jnp.zeros_like(high)
        high_row = jnp.dot(ones, jnp.where(eye, high, zero), preferred_element_type=f32)
        low_row = jnp.dot(ones, jnp.where(eye, low, zero), preferred_element_type=f32)
        out_ref[s, HALF:, :] = jnp.where(sub == 0, high_row, low_row).astype(bf16)
        return carry

    lax.fori_loop(0, PLANE, merge, 0)


def plane_attention(z, kv, q, halo):
    vmem = pl.BlockSpec(memory_space=pltpu.VMEM)
    scratch = pltpu.VMEM((PLANE, HALF, HEAD), f32)
    return pl.pallas_call(
        plane_kernel,
        in_specs=[pl.BlockSpec(memory_space=pltpu.SMEM), vmem, vmem, vmem],
        out_specs=vmem,
        out_shape=jax.ShapeDtypeStruct((PLANE, RETURN_ROWS, HEAD), bf16),
        scratch_shapes=[scratch] * 4,
        compiler_params=pltpu.CompilerParams(vmem_limit_bytes=20 * 2**20),
        cost_estimate=pl.CostEstimate(flops=32 * 4 * 128 * 256 * 128, bytes_accessed=5 * 2**20, transcendentals=2**20),
        name="plane_attention",
    )(z, kv, q, halo)


def near_kernel(z_ref, cos_ref, sin_ref, pcos_ref, psin_ref, q_ref, k_ref, v_ref, halo_ref, out_ref, log_ref):
    bias = jnp.where(z_ref[0] == 0, MASKED, -MASKED)
    cosine, sine = full_tables(cos_ref, sin_ref)
    pcos, psin = full_tables(pcos_ref, psin_ref)
    lane = iota((TOKENS, HEAD), 1)

    def head(h, held):
        lanes = pl.ds(pl.multiple_of(h * HEAD, HEAD), HEAD)
        q = (turned(q_ref[:, lanes], cosine, sine) * SCALE).astype(bf16)
        k = turned(k_ref[:, lanes], cosine, sine).astype(bf16)
        v = v_ref[:, lanes]
        ks = [turned(halo_ref[0, :, lanes], pcos, psin).astype(bf16), k[:HALF], k[HALF:]]
        vs = [halo_ref[1, :, lanes], v[:HALF], v[HALF:]]
        parts = []
        for b in range(2):
            result, logs = attend(
                q[b * HALF : (b + 1) * HALF], ks[b], ks[b + 1], vs[b], vs[b + 1], bias if b == 0 else None
            )
            out_ref[b * HALF : (b + 1) * HALF, lanes] = result
            parts.append(wide(logs))
        return jnp.where(lane == h, jnp.concatenate(parts, axis=0), held)

    log_ref[...] = lax.fori_loop(0, LOCAL, head, jnp.zeros((TOKENS, HEAD), f32))


def near_attention(device, cosine, sine, pcos, psin, queries, keys, values, halo):
    vmem = pl.BlockSpec(memory_space=pltpu.VMEM)
    group0 = pl.BlockSpec((None, TOKENS, LOCAL * HEAD), lambda i: (0, 0, 0))
    full = lambda *shape: pl.BlockSpec(shape, lambda i: (0,) * len(shape))
    return pl.pallas_call(
        near_kernel,
        grid=(1,),
        in_specs=[
            pl.BlockSpec(memory_space=pltpu.SMEM),
            full(TOKENS, HEAD // 2),
            full(TOKENS, HEAD // 2),
            full(HALF, HEAD // 2),
            full(HALF, HEAD // 2),
            group0,
            group0,
            group0,
            full(2, HALF, LOCAL * HEAD),
        ],
        out_specs=[full(TOKENS, LOCAL * HEAD), full(TOKENS, HEAD)],
        out_shape=[
            jax.ShapeDtypeStruct((TOKENS, LOCAL * HEAD), f32),
            jax.ShapeDtypeStruct((TOKENS, HEAD), f32),
        ],
        cost_estimate=pl.CostEstimate(flops=16 * 4 * 128 * 256 * 128, bytes_accessed=4 * 2**20, transcendentals=2**19),
        name="near_attention",
    )(device, cosine, sine, pcos, psin, queries, keys, values, halo)


def merge_kernel(near_ref, log_ref, far_ref, out_ref, far, far_log):
    eye = iota((HALF, HEAD), 0) == iota((HALF, HEAD), 1)
    ones = jnp.ones((HEAD, HEAD), bf16)
    for h in range(LOCAL):
        lanes = slice(h * HEAD, (h + 1) * HEAD)
        for p in range(2):
            piece = 2 * h + p
            target = pl.ds(p, HALF, stride=2)
            far[target, :] = far_ref[piece, :HALF, :].astype(f32)
            logs = far_ref[piece, HALF:, :]
            zero = jnp.zeros((HALF, HEAD), bf16)
            high = jnp.where(eye, jnp.broadcast_to(logs[0:1, :], (HALF, HEAD)), zero)
            low = jnp.where(eye, jnp.broadcast_to(logs[1:2, :], (HALF, HEAD)), zero)
            far_log[target, :] = jnp.dot(high, ones, preferred_element_type=f32) + jnp.dot(
                low, ones, preferred_element_type=f32
            )
        l0 = wide(log_ref[:, h : h + 1])
        l12 = far_log[...]
        m = jnp.maximum(l0, l12)
        e0, e12 = jnp.exp(l0 - m), jnp.exp(l12 - m)
        out_ref[:, lanes] = ((e0 * near_ref[:, lanes] + e12 * far[...]) / (e0 + e12)).astype(bf16)


def merge_groups(near, log, far):
    vmem = pl.BlockSpec(memory_space=pltpu.VMEM)
    return pl.pallas_call(
        merge_kernel,
        in_specs=[vmem] * 3,
        out_specs=vmem,
        out_shape=jax.ShapeDtypeStruct((TOKENS, LOCAL * HEAD), bf16),
        scratch_shapes=[pltpu.VMEM((TOKENS, HEAD), f32)] * 2,
        compiler_params=pltpu.CompilerParams(vmem_limit_bytes=8 * 2**20),
        cost_estimate=pl.CostEstimate(flops=2**24, bytes_accessed=2**21, transcendentals=2**19),
        name="merge_groups",
    )(near, log, far)


def project_kernel(core_ref, mine_ref, other_ref, w_ref, out_ref):
    half = LOCAL * HEAD
    core = core_ref[0]
    mine = pl.ds(pl.multiple_of(core * half, half), half)
    other = pl.ds(pl.multiple_of((1 - core) * half, half), half)
    total = jnp.dot(mine_ref[...], w_ref[mine, :], preferred_element_type=f32)
    total += jnp.dot(other_ref[...], w_ref[other, :], preferred_element_type=f32)
    out_ref[...] = total.astype(bf16)


def project(core, mine, other, w_out):
    vmem = pl.BlockSpec(memory_space=pltpu.VMEM)
    return pl.pallas_call(
        project_kernel,
        in_specs=[pl.BlockSpec(memory_space=pltpu.SMEM), vmem, vmem, vmem],
        out_specs=vmem,
        out_shape=jax.ShapeDtypeStruct((TOKENS, w_out.shape[1]), bf16),
        compiler_params=pltpu.CompilerParams(vmem_limit_bytes=16 * 2**20),
        cost_estimate=pl.CostEstimate(flops=2**30, bytes_accessed=2**22, transcendentals=0),
        name="project",
    )(core, mine, other, w_out)


def tables(count, start):
    inverse = ROPE_BASE ** (-jnp.arange(0, HEAD, 2, dtype=f32) / HEAD)
    angles = (lax.iota(jnp.int32, count) + start).astype(f32)[:, None] * inverse[None, :]
    return jnp.cos(angles), jnp.sin(angles)


def shards(queries, keys, values, w_out):
    devices = lax.axis_size("sp")
    assert queries.shape == (3, TOKENS, LOCAL * HEAD) and devices % PLANE == 0
    planes = [[p * PLANE + i for i in range(PLANE)] for p in range(devices // PLANE)]
    exchange = functools.partial(
        lax.all_to_all, axis_name="sp", split_axis=0, concat_axis=0, axis_index_groups=planes, tiled=True
    )
    device = lax.axis_index("sp")
    core = lax.axis_index("tp").reshape(1)
    start = device * TOKENS
    edge = jnp.stack([keys[0, HALF:], values[0, HALF:]])
    cosine, sine = tables(TOKENS, start)
    cosine, sine, edge = lax.optimization_barrier((cosine, sine, edge))
    edge = lax.ppermute(edge, "sp", [(i, i + 1) for i in range(devices - 1)])

    kv = prepare(((1, "k"), (1, "v"), (2, "k"), (2, "v")), (keys, values, keys, values), cosine, sine)
    kv = exchange(kv)
    q = prepare(((1, "q"), (2, "q")), (queries, queries), cosine, sine)
    pcos, psin = tables(HALF, start - HALF)
    near, log = near_attention(device.reshape(1), cosine, sine, pcos, psin, queries, keys, values, edge)
    near, log, q = lax.optimization_barrier((near, log, q))
    q = exchange(q)
    behind = jnp.concatenate(
        [
            kv[PLANE // 2 :, 2:].reshape(PLANE, HALF, HEAD),
            kv[PLANE - 2 :, :2].reshape(4, HALF, HEAD),
        ]
    )
    halo = lax.ppermute(behind, "sp", [(i, i + PLANE) for i in range(devices - PLANE)])

    far = exchange(plane_attention((device // PLANE).reshape(1), kv, q, halo))
    attended = merge_groups(near, log, far)
    other = lax.ppermute(attended, "tp", [(0, 1), (1, 0)])
    return project(core, attended, other, w_out)


def solution(mesh):
    return jax.shard_map(
        shards,
        mesh=mesh,
        in_specs=(P(None, "sp", "tp"), P(None, "sp", "tp"), P(None, "sp", "tp"), P(None, "tp")),
        out_specs=P("sp", "tp"),
        check_vma=False,
    )
```

profile of v0, /device:TPU:137, one launch (start us, length us, event | category | flops | bytes accessed | tf_op | source)
XLA Modules:
  0.0 129.6 jit_solution(5736570313769518262)
XLA Ops:
  0.0 1.0 slice.12
  1.0 1.0 slice.13
  2.0 1.3 multiply_sine_fusion
  3.2 0.1 pad_maximum_fusion.1
  3.3 5.0 %shard_map.47 = bf16[16,4,128,128]{3,2,1,0:T(8,128)(2,1)} custom-call(f32[256,64]{1,0:T(8,128)} %get-tuple-element.13.cos_ref.refs_0_, f32[256,64]{1,0:T(8,128)} %get-tuple-element.14.sin_ref.refs_1_, bf16[3,256,1024]{2,1,0:T(8,128)(2,1)} %refs_4_.1, bf16[3,256,1024]{2,1,0:T(8,128)(2,1)} %refs_5_.1, bf16[3,256,1024]{2,1,0:T(8,128)(2,1)} %refs_4_.1, ...), custom_call_target="tpu_custom_call" | custom-call | flops 2147483648 | bytes 4194304 | tf_op jit(solution)/shard_map/pallas_call | solution.py:80
  8.3 6.8 %all-to-all-start = ((bf16[16,4,128,128]{3,2,1,0:T(8,128)(2,1)}), bf16[16,4,128,128]{3,2,1,0:T(8,128)(2,1)S(1)}, u32[]{:S(2)}, u32[]{:S(2)}) async-start(bf16[16,4,128,128]{3,2,1,0:T(8,128)(2,1)} %shard_map.47), calls=%async_computation | async-start | bytes 4194304 | tf_op jit(solution)/shard_map/all_to_all | solution.py:341
  15.1 3.1 %collective-permute-start = (bf16[2,128,1024]{2,1,0:T(8,128)(2,1)S(1)}, bf16[2,128,1024]{2,1,0:T(8,128)(2,1)S(1)}, u32[]{:S(2)}, u32[]{:S(2)}) collective-permute-start(bf16[2,128,1024]{2,1,0:T(8,128)(2,1)S(1)} %pad_maximum_fusion.1), channel_id=1, source_target_pairs={{0,2},{2,4},{4,6},{6,8},{8,10},{10,12},{12,14},{14,16},{16,18},{18... | collective-permute-start | bytes 1572872 | tf_op jit(solution)/shard_map/ppermute | solution.py:338
  18.2 4.5 %shard_map.46 = bf16[16,2,128,128]{3,2,1,0:T(8,128)(2,1)} custom-call(f32[256,64]{1,0:T(8,128)} %get-tuple-element.13.cos_ref.refs_0_, f32[256,64]{1,0:T(8,128)} %get-tuple-element.14.sin_ref.refs_1_, bf16[3,256,1024]{2,1,0:T(8,128)(2,1)} %refs_3_.2, bf16[3,256,1024]{2,1,0:T(8,128)(2,1)} %refs_3_.2), custom_call_target="tpu_custom_call" | custom-call | flops 1073741824 | bytes 2097152 | tf_op jit(solution)/shard_map/pallas_call | solution.py:80
  22.7 1.0 multiply_sine_fusion.1
  23.6 31.2 %collective-permute-done.halo_ref = bf16[2,128,1024]{2,1,0:T(8,128)(2,1)S(1)} collective-permute-done((bf16[2,128,1024]{2,1,0:T(8,128)(2,1)S(1)}, bf16[2,128,1024]{2,1,0:T(8,128)(2,1)S(1)}, u32[]{:S(2)}, u32[]{:S(2)}) %collective-permute-start) | collective-permute-done | bytes 524320 | tf_op jit(solution)/shard_map/ppermute | solution.py:338
  54.9 0.0 copy-start.3
  54.9 0.8 copy-done.3
  55.7 8.8 %near_attention.1 = (f32[256,1024]{1,0:T(8,128)}, f32[256,128]{1,0:T(8,128)}) custom-call(s32[1]{0:T(128)} %bitcast.1.z_ref, f32[256,64]{1,0:T(8,128)} %get-tuple-element.13.cos_ref.refs_0_, f32[256,64]{1,0:T(8,128)} %get-tuple-element.14.sin_ref.refs_1_, f32[128,64]{1,0:T(8,128)} %get-tuple-element.24.pcos_ref, f32[128,64]{1,0:T(8,128)} %get-tuple-element.23.psin_ref, ...), custom_call_target="tpu_custom_call" | custom-call | flops 268435456 | bytes 4194304 | tf_op jit(solution)/shard_map/near_attention/pallas_call | solution.py:235
  64.5 0.0 all-to-all-done.kv_ref
  64.5 6.3 %all-to-all-start.1 = ((bf16[16,2,128,128]{3,2,1,0:T(8,128)(2,1)}), bf16[16,2,128,128]{3,2,1,0:T(8,128)(2,1)S(1)}, u32[]{:S(2)}, u32[]{:S(2)}) async-start(bf16[16,2,128,128]{3,2,1,0:T(8,128)(2,1)} %shard_map.46), calls=%async_computation.1 | async-start | bytes 2097152 | tf_op jit(solution)/shard_map/all_to_all | solution.py:346
  70.8 0.9 pad_maximum_fusion
  71.7 2.6 %collective-permute-start.1 = (bf16[20,128,128]{2,1,0:T(8,128)(2,1)}, bf16[20,128,128]{2,1,0:T(8,128)(2,1)}, u32[]{:S(2)}, u32[]{:S(2)}) collective-permute-start(bf16[20,128,128]{2,1,0:T(8,128)(2,1)} %pad_maximum_fusion), channel_id=1, source_target_pairs={{0,32},{2,34},{4,36},{6,38},{8,40},{10,42},{12,44},{14,46},{16,48}... | collective-permute-start | bytes 1966088 | tf_op jit(solution)/shard_map/ppermute | solution.py:353
  74.3 10.5 %all-to-all-done.1.q_ref = bf16[16,2,128,128]{3,2,1,0:T(8,128)(2,1)S(1)} async-done(((bf16[16,2,128,128]{3,2,1,0:T(8,128)(2,1)}), bf16[16,2,128,128]{3,2,1,0:T(8,128)(2,1)S(1)}, u32[]{:S(2)}, u32[]{:S(2)}) %all-to-all-start.1) | async-done | bytes 1048608 | tf_op jit(solution)/shard_map/all_to_all | solution.py:346
  84.8 4.3 %collective-permute-done.1.halo_ref = bf16[20,128,128]{2,1,0:T(8,128)(2,1)} collective-permute-done((bf16[20,128,128]{2,1,0:T(8,128)(2,1)}, bf16[20,128,128]{2,1,0:T(8,128)(2,1)}, u32[]{:S(2)}, u32[]{:S(2)}) %collective-permute-start.1) | collective-permute-done | bytes 655392 | tf_op jit(solution)/shard_map/ppermute | solution.py:353
  89.1 0.0 copy-start.1
  89.1 0.0 copy-start.2
  89.1 14.6 %plane_attention.1 = bf16[16,144,128]{2,1,0:T(8,128)(2,1)S(1)} custom-call(s32[1]{0:T(128)} %bitcast.2.z_ref, bf16[16,4,128,128]{3,2,1,0:T(8,128)(2,1)S(1)} %all-to-all-done.kv_ref, bf16[16,2,128,128]{3,2,1,0:T(8,128)(2,1)S(1)} %all-to-all-done.1.q_ref, bf16[20,128,128]{2,1,0:T(8,128)(2,1)} %collective-permute-done.1.halo_ref), custom_call_target="tpu_custom_call" | custom-call | flops 536870912 | bytes 5242880 | tf_op jit(solution)/shard_map/plane_attention/pallas_call | solution.py:194
  103.6 14.8 %all_to_all.15.far_ref = bf16[16,144,128]{2,1,0:T(8,128)(2,1)S(1)} all-to-all(bf16[16,144,128]{2,1,0:T(8,128)(2,1)S(1)} %plane_attention.1), channel_id=1, replica_groups={{0,2,4,6,8,10,12,14,16,18,20,22,24,26,28,30},{32,34,36,38,40,42,44,46,4..., dimensions={0} | all-to-all | bytes 1179648 | tf_op jit(solution)/shard_map/all_to_all | solution.py:355
  118.4 0.0 copy-done.1
  118.4 0.0 copy-done.2
  118.4 0.8 merge_groups.1.mine_ref
  119.2 4.6 %collective-permute-start.2 = (bf16[256,1024]{1,0:T(8,128)(2,1)S(1)}, bf16[256,1024]{1,0:T(8,128)(2,1)S(1)}, u32[]{:S(2)}, u32[]{:S(2)}) collective-permute-start(bf16[256,1024]{1,0:T(8,128)(2,1)S(1)} %merge_groups.1.mine_ref), channel_id=1, source_target_pairs={{0,1},{1,0},{2,3},{3,2},{4,5},{5,4},{6,7},{7,6},{8,9},{9,8},{10,11... | collective-permute-start | bytes 1572872 | tf_op jit(solution)/shard_map/ppermute | solution.py:357
  123.8 1.5 %collective-permute-done.2.other_ref = bf16[256,1024]{1,0:T(8,128)(2,1)S(1)} collective-permute-done((bf16[256,1024]{1,0:T(8,128)(2,1)S(1)}, bf16[256,1024]{1,0:T(8,128)(2,1)S(1)}, u32[]{:S(2)}, u32[]{:S(2)}) %collective-permute-start.2) | collective-permute-done | bytes 524320 | tf_op jit(solution)/shard_map/ppermute | solution.py:357
  125.4 0.0 copy-start
  125.4 2.2 %copy-done = bf16[2048,1024]{1,0:T(8,128)(2,1)S(1)} copy-done((bf16[2048,1024]{1,0:T(8,128)(2,1)S(1)}, bf16[2048,1024]{1,0:T(8,128)(2,1)}, u32[]{:S(2)}) %copy-start) | copy-done | bytes 4194328
  127.6 2.0 %project.1 = bf16[256,1024]{1,0:T(8,128)(2,1)} custom-call(s32[1]{0:T(128)} %bitcast.core_ref, bf16[256,1024]{1,0:T(8,128)(2,1)S(1)} %merge_groups.1.mine_ref, bf16[256,1024]{1,0:T(8,128)(2,1)S(1)} %collective-permute-done.2.other_ref, bf16[2048,1024]{1,0:T(8,128)(2,1)S(1)} %copy-done), custom_call_target="tpu_custom_call" | custom-call | flops 1073741824 | bytes 4194304 | tf_op jit(solution)/shard_map/project/pallas_call | solution.py:308
  (5 shorter events, 0.1 us)
Async XLA Ops:
  8.3 56.2 %all-to-all-start = ((bf16[16,4,128,128]{3,2,1,0:T(8,128)(2,1)}), bf16[16,4,128,128]{3,2,1,0:T(8,128)(2,1)S(1)}, u32[]{:S(2)}, u32[]{:S(2)}) async-start(bf16[16,4,128,128]{3,2,1,0:T(8,128)(2,1)} %shard_map.47), calls=%async_computation | async-start | bytes 4194304 | tf_op jit(solution)/shard_map/all_to_all | solution.py:341
  15.1 39.8 %collective-permute-start = (bf16[2,128,1024]{2,1,0:T(8,128)(2,1)S(1)}, bf16[2,128,1024]{2,1,0:T(8,128)(2,1)S(1)}, u32[]{:S(2)}, u32[]{:S(2)}) collective-permute-start(bf16[2,128,1024]{2,1,0:T(8,128)(2,1)S(1)} %pad_maximum_fusion.1), channel_id=1, source_target_pairs={{0,2},{2,4},{4,6},{6,8},{8,10},{10,12},{12,14},{14,16},{16,18},{18... | collective-permute-start | bytes 1572872 | tf_op jit(solution)/shard_map/ppermute | solution.py:338
  54.9 0.8 copy-start.3
  64.5 20.3 %all-to-all-start.1 = ((bf16[16,2,128,128]{3,2,1,0:T(8,128)(2,1)}), bf16[16,2,128,128]{3,2,1,0:T(8,128)(2,1)S(1)}, u32[]{:S(2)}, u32[]{:S(2)}) async-start(bf16[16,2,128,128]{3,2,1,0:T(8,128)(2,1)} %shard_map.46), calls=%async_computation.1 | async-start | bytes 2097152 | tf_op jit(solution)/shard_map/all_to_all | solution.py:346
  71.7 17.4 %collective-permute-start.1 = (bf16[20,128,128]{2,1,0:T(8,128)(2,1)}, bf16[20,128,128]{2,1,0:T(8,128)(2,1)}, u32[]{:S(2)}, u32[]{:S(2)}) collective-permute-start(bf16[20,128,128]{2,1,0:T(8,128)(2,1)} %pad_maximum_fusion), channel_id=1, source_target_pairs={{0,32},{2,34},{4,36},{6,38},{8,40},{10,42},{12,44},{14,46},{16,48}... | collective-permute-start | bytes 1966088 | tf_op jit(solution)/shard_map/ppermute | solution.py:353
  89.1 29.4 %copy-start.1 = (f32[256,1024]{1,0:T(8,128)S(1)}, f32[256,1024]{1,0:T(8,128)}, u32[]{:S(2)}) copy-start(f32[256,1024]{1,0:T(8,128)} %get-tuple-element.18.near_ref) | copy-start | bytes 3145732
  89.1 29.4 %copy-start.2 = (f32[256,128]{1,0:T(8,128)S(1)}, f32[256,128]{1,0:T(8,128)}, u32[]{:S(2)}) copy-start(f32[256,128]{1,0:T(8,128)} %get-tuple-element.19.log_ref) | copy-start | bytes 393220
  119.2 6.1 %collective-permute-start.2 = (bf16[256,1024]{1,0:T(8,128)(2,1)S(1)}, bf16[256,1024]{1,0:T(8,128)(2,1)S(1)}, u32[]{:S(2)}, u32[]{:S(2)}) collective-permute-start(bf16[256,1024]{1,0:T(8,128)(2,1)S(1)} %merge_groups.1.mine_ref), channel_id=1, source_target_pairs={{0,1},{1,0},{2,3},{3,2},{4,5},{5,4},{6,7},{7,6},{8,9},{9,8},{10,11... | collective-permute-start | bytes 1572872 | tf_op jit(solution)/shard_map/ppermute | solution.py:357
  125.4 2.2 %copy-start = (bf16[2048,1024]{1,0:T(8,128)(2,1)S(1)}, bf16[2048,1024]{1,0:T(8,128)(2,1)}, u32[]{:S(2)}) copy-start(bf16[2048,1024]{1,0:T(8,128)(2,1)} %w_ref.1) | copy-start | bytes 12582916
where the time goes:
time: 131 us; the launch traced here: 130 us
  waiting for transfers between devices  47.5 us (36%)
  Pallas kernels  35.6 us (27%)
  starting transfers between devices  23.4 us (18%)
  blocking collectives  14.8 us (11%)
  local copies, waits for them, and re-layouts  4.97 us (4%)
  other arithmetic  3.2 us (2%)
    ppermute x1, waiting for transfers between devices, shards(): edge = lax.ppermute(edge, 'sp', [(i, i + 1) for i in range(devices - 1)])  31.2 us
    all_to_all x1, blocking collectives, shards(): far = exchange(plane_attention((device // PLANE).reshape(1), kv, q, halo))  14.8 us
    pallas_call x1, Pallas kernels, plane_attention(): pl.pallas_call(plane_kernel, in_specs=[pl.BlockSpec(memory_space=pltpu.SM...  14.6 us
    all_to_all x1, waiting for transfers between devices, shards(): q = exchange(q)  10.5 us
    pallas_call x2, Pallas kernels, prepare(): pl.pallas_call(functools.partial(prepare_kernel, kinds), grid=(LOCAL // 2...  9.46 us
    pallas_call x1, Pallas kernels, near_attention(): pl.pallas_call(near_kernel, grid=(1,), in_specs=[pl.BlockSpec(memory_spac...  8.77 us
    all_to_all x1, starting transfers between devices, shards(): kv = exchange(kv)  6.83 us
    all_to_all x1, starting transfers between devices, shards(): q = exchange(q)  6.27 us
  transfers between devices with their start and end apart: 5, of which 4 were waited for; matrix products, arithmetic and copies ran while one was open for 1% of the time, Pallas kernels for 10%

commit v1 on v0

v1 whole, which is shorter than its diff:
```python
import functools

import jax
import jax.numpy as jnp
from jax import lax
from jax.experimental import pallas as pl
from jax.experimental.pallas import tpu as pltpu
from jax.sharding import PartitionSpec as P


HEAD = 128
WINDOW = 128
ROPE_BASE = 10000.0
MASKED = -1e30
SCALE = HEAD ** (-0.5)

TOKENS = 256
LOCAL = 8
PLANE = 16
HALF = TOKENS // 2
ROW = 4
ROW_HEADS = LOCAL // ROW
STRIDES = {1: 4, 2: 16}
RETURN_ROWS = HALF + 16
ROW_RETURN = TOKENS + 16


f32 = jnp.float32
bf16 = jnp.bfloat16


def iota(shape, dim):
    return lax.broadcasted_iota(jnp.int32, shape, dim)


def turned(x, cosine, sine):
    x = x.astype(f32)
    return x * cosine + pltpu.roll(x, HEAD // 2, 1) * sine


def full_tables(cos_ref, sin_ref):
    cosine, sine = cos_ref[...], sin_ref[...]
    return jnp.concatenate([cosine, cosine], axis=1), jnp.concatenate([-sine, sine], axis=1)


def sorting(group):
    row = iota((TOKENS, TOKENS), 0)
    token = iota((TOKENS, TOKENS), 1)
    stride = STRIDES[group]
    steps = TOKENS // stride
    if group == 2:
        within = row % HALF
        picked = row // HALF + 2 * (within // steps) + stride * (within % steps)
    else:
        picked = row // steps + stride * (row % steps)
    return jnp.where(picked == token, 1.0, 0.0).astype(bf16)


def prepare_kernel(group, kinds, me_ref, *refs):
    cos_ref, sin_ref = refs[:2]
    ins, out_ref, sort_ref, full_ref = refs[2:-3], refs[-3], refs[-2], refs[-1]

    @pl.when(pl.program_id(0) == 0)
    def _():
        sort_ref[...] = sorting(group)
        full_ref[0], full_ref[1] = full_tables(cos_ref, sin_ref)

    cosine, sine = full_ref[0], full_ref[1]
    for a, kind in enumerate(kinds):
        x = ins[a][...]
        if kind != "v":
            heads = [turned(x[:, h * HEAD : (h + 1) * HEAD], cosine, sine) for h in range(2)]
            if kind == "q":
                heads = [x * SCALE for x in heads]
            x = jnp.concatenate([x.astype(bf16) for x in heads], axis=1)
        y = jnp.dot(sort_ref[...], x, preferred_element_type=f32).astype(bf16)
        for h in range(2):
            lanes = slice(h * HEAD, (h + 1) * HEAD)
            if group == 2:
                for p in range(2):
                    out_ref[2 * h + p, a] = y[p * HALF : (p + 1) * HALF, lanes]
            else:
                out_ref[a, h] = y[:, lanes]


def prepare(group, kinds, arrays, me, cosine, sine):
    n = len(kinds)
    table = pl.BlockSpec((TOKENS, HEAD // 2), lambda g, me: (0, 0))
    if group == 2:
        out_spec = pl.BlockSpec((4, n, HALF, HEAD), lambda g, me: (g, 0, 0, 0))
        out_shape = (PLANE, n, HALF, HEAD)
    else:
        out_spec = pl.BlockSpec(
            (None, n, ROW_HEADS, TOKENS, HEAD), lambda g, me: (lax.rem(g + ROW - me[0], ROW), 0, 0, 0, 0)
        )
        out_shape = (ROW, n, ROW_HEADS, TOKENS, HEAD)
    return pl.pallas_call(
        functools.partial(prepare_kernel, group, kinds),
        grid_spec=pltpu.PrefetchScalarGridSpec(
            num_scalar_prefetch=1,
            grid=(LOCAL // 2,),
            in_specs=[table, table]
            + [pl.BlockSpec((None, TOKENS, 2 * HEAD), lambda g, me: (group, 0, g)) for _ in kinds],
            out_specs=out_spec,
            scratch_shapes=[pltpu.VMEM((TOKENS, TOKENS), bf16), pltpu.VMEM((2, TOKENS, HEAD), f32)],
        ),
        out_shape=jax.ShapeDtypeStruct(out_shape, bf16),
        cost_estimate=pl.CostEstimate(
            flops=n * LOCAL * 2 * TOKENS * TOKENS * HEAD * 4, bytes_accessed=n * 2**20, transcendentals=0
        ),
    )(me, cosine, sine, *arrays)


def dot_t(a, b):
    return lax.dot_general(a, b, (((1,), (1,)), ((), ())), preferred_element_type=f32)


def attend(q, k_prev, k_cur, v_prev, v_cur, prev_bias):
    row = iota((WINDOW, 2 * WINDOW), 0)
    col = iota((WINDOW, 2 * WINDOW), 1)
    scores = dot_t(q, jnp.concatenate([k_prev, k_cur], axis=0))
    scores = jnp.where((col >= row) & (col <= row + WINDOW), scores, MASKED)
    if prev_bias is not None:
        scores = jnp.minimum(scores, jnp.where(iota((1, 2 * WINDOW), 1) < WINDOW, prev_bias, -MASKED))
    row_max = jnp.max(scores, axis=1, keepdims=True)
    probs = jnp.exp(scores - row_max)
    row_sum = jnp.sum(probs, axis=1, keepdims=True)
    total = jnp.dot(probs.astype(bf16), jnp.concatenate([v_prev, v_cur], axis=0), preferred_element_type=f32)
    return total / row_sum, row_max + jnp.log(row_sum)


def wide(column):
    return jnp.broadcast_to(column, (column.shape[0], HEAD))


def column_to_rows(column):
    eye = iota((HALF, HEAD), 0) == iota((HALF, HEAD), 1)
    ones = jnp.ones((16, HALF), bf16)
    column = wide(column)
    high = column.astype(bf16)
    low = (column - high.astype(f32)).astype(bf16)
    zero = jnp.zeros_like(high)
    high = jnp.dot(ones, jnp.where(eye, high, zero), preferred_element_type=f32)
    low = jnp.dot(ones, jnp.where(eye, low, zero), preferred_element_type=f32)
    return jnp.where(iota((16, HEAD), 0) % 2 == 0, high, low)


def rows_to_column(high, low):
    eye = iota((HALF, HEAD), 0) == iota((HALF, HEAD), 1)
    ones = jnp.ones((HEAD, HEAD), bf16)
    zero = jnp.zeros((HALF, HEAD), bf16)
    return sum(
        jnp.dot(jnp.where(eye, jnp.broadcast_to(part, (HALF, HEAD)), zero), ones, preferred_element_type=f32)
        for part in (high, low)
    )


def plane_kernel(z_ref, kv_ref, q_ref, halo_ref, out_ref, logs_ref):
    bias = jnp.where(z_ref[0] == 0, MASKED, -MASKED)
    for r in range(8):
        rows = slice(r * 16, (r + 1) * 16)
        ks = [jnp.concatenate([halo_ref[i, 0, rows, :] for i in range(8)], axis=0)]
        vs = [jnp.concatenate([halo_ref[i, 1, rows, :] for i in range(8)], axis=0)]
        for b in range(2):
            chips = range(8 * b, 8 * b + 8)
            ks.append(jnp.concatenate([kv_ref[s, 0, rows, :] for s in chips], axis=0))
            vs.append(jnp.concatenate([kv_ref[s, 1, rows, :] for s in chips], axis=0))
            q = jnp.concatenate([q_ref[s, 0, rows, :] for s in chips], axis=0)
            result, logs = attend(q, ks[b], ks[b + 1], vs[b], vs[b + 1], bias if b == 0 else None)
            for i, s in enumerate(chips):
                out_ref[s, rows, :] = result[i * 16 : (i + 1) * 16].astype(bf16)
                logs_ref[s, rows, :] = logs[i * 16 : (i + 1) * 16]
    for s in range(PLANE):
        out_ref[s, HALF:, :] = column_to_rows(logs_ref[s]).astype(bf16)


def plane_attention(z, kv, q, halo):
    vmem = pl.BlockSpec(memory_space=pltpu.VMEM)
    return pl.pallas_call(
        plane_kernel,
        in_specs=[pl.BlockSpec(memory_space=pltpu.SMEM), vmem, vmem, vmem],
        out_specs=vmem,
        out_shape=jax.ShapeDtypeStruct((PLANE, RETURN_ROWS, HEAD), bf16),
        scratch_shapes=[pltpu.VMEM((PLANE, HALF, 1), f32)],
        compiler_params=pltpu.CompilerParams(vmem_limit_bytes=20 * 2**20),
        cost_estimate=pl.CostEstimate(flops=2**31, bytes_accessed=3 * 2**20, transcendentals=2**19),
        name="plane_attention",
    )(z, kv, q, halo)


def pick_kernel(x_ref, own_ref, one_ref, two_ref, three_ref, out_ref):
    x = x_ref[0]
    for steps, ref in enumerate((own_ref, one_ref, two_ref, three_ref)):
        chip = lax.rem(x + ROW - steps, ROW)

        @pl.when(chip >= ROW // 2)
        def _(ref=ref, chip=chip):
            out_ref[chip - ROW // 2] = ref[:2]


def row_specs(own, others):
    piece = own.shape[1:]
    whole = lambda shape: pl.BlockSpec(shape, lambda i: (0,) * len(shape))
    return [pl.BlockSpec((None, *piece), lambda i: (0,) * (len(piece) + 1))] + [whole(o.shape) for o in others]


def pick_last(x, own, others):
    shape = (2, 2, ROW_HEADS, TOKENS, HEAD)
    return pl.pallas_call(
        pick_kernel,
        grid=(1,),
        in_specs=[pl.BlockSpec(memory_space=pltpu.SMEM)] + row_specs(own, others),
        out_specs=pl.BlockSpec(shape, lambda i: (0,) * 5),
        out_shape=jax.ShapeDtypeStruct(shape, bf16),
        cost_estimate=pl.CostEstimate(flops=2**20, bytes_accessed=2**21, transcendentals=0),
        name="pick_last",
    )(x, own, *others)


def row_kernel(x_ref, own_ref, one_ref, two_ref, three_ref, halo_ref, *refs):
    outs, in_ref, res_ref = refs[:4], refs[4], refs[5]
    x = x_ref[0]
    bias = jnp.where(x_ref[1] == 0, MASKED, -MASKED)
    for steps, ref in enumerate((own_ref, one_ref, two_ref, three_ref)):
        in_ref[lax.rem(x + ROW - steps, ROW)] = ref[...]
    for h in range(ROW_HEADS):
        for r in range(4):
            rows = slice(r * 64, (r + 1) * 64)
            ks = [jnp.concatenate([halo_ref[i, 0, h, rows, :] for i in range(2)], axis=0)]
            vs = [jnp.concatenate([halo_ref[i, 1, h, rows, :] for i in range(2)], axis=0)]
            for b in range(2):
                chips = (2 * b, 2 * b + 1)
                ks.append(jnp.concatenate([in_ref[s, 0, h, rows, :] for s in chips], axis=0))
                vs.append(jnp.concatenate([in_ref[s, 1, h, rows, :] for s in chips], axis=0))
                q = jnp.concatenate([in_ref[s, 2, h, rows, :] for s in chips], axis=0)
                result, logs = attend(q, ks[b], ks[b + 1], vs[b], vs[b + 1], bias if b == 0 else None)
                tile = column_to_rows(logs)
                for i, s in enumerate(chips):
                    res_ref[s, h, rows, :] = result[i * 64 : (i + 1) * 64].astype(bf16)
                    half = tile if i == 0 else pltpu.roll(tile, HEAD // 2, 1)
                    sub = iota((16, HEAD), 0)
                    held = half if r == 0 else jnp.where(sub // 2 == r, half, carried[i + 2 * b])
                    if r == 0 and b == 0 and i == 0:
                        carried = {}
                    carried[i + 2 * b] = held
                    if r == 3:
                        res_ref[s, h, TOKENS:, :] = held.astype(bf16)
    for steps, out in enumerate(outs):
        out[...] = res_ref[lax.rem(x + steps, ROW)]


def row_attention(place, own, others, halo):
    shape = (ROW_HEADS, ROW_RETURN, HEAD)
    return pl.pallas_call(
        row_kernel,
        grid=(1,),
        in_specs=[pl.BlockSpec(memory_space=pltpu.SMEM)]
        + row_specs(own, others)
        + [pl.BlockSpec(halo.shape, lambda i: (0,) * 5)],
        out_specs=[pl.BlockSpec(shape, lambda i: (0,) * 3)] * ROW,
        out_shape=[jax.ShapeDtypeStruct(shape, bf16)] * ROW,
        scratch_shapes=[
            pltpu.VMEM((ROW, 3, ROW_HEADS, TOKENS, HEAD), bf16),
            pltpu.VMEM((ROW, *shape), bf16),
        ],
        cost_estimate=pl.CostEstimate(flops=2**31, bytes_accessed=3 * 2**20, transcendentals=2**19),
        name="row_attention",
    )(place, own, *others, halo)


def near_kernel(z_ref, cos_ref, sin_ref, pcos_ref, psin_ref, q_ref, k_ref, v_ref, halo_ref, out_ref, log_ref):
    bias = jnp.where(z_ref[0] == 0, MASKED, -MASKED)
    cosine, sine = full_tables(cos_ref, sin_ref)
    pcos, psin = full_tables(pcos_ref, psin_ref)
    lane = iota((TOKENS, HEAD), 1)

    held = jnp.zeros((TOKENS, HEAD), f32)
    for h in range(LOCAL):
        lanes = slice(h * HEAD, (h + 1) * HEAD)
        q = (turned(q_ref[:, lanes], cosine, sine) * SCALE).astype(bf16)
        k = turned(k_ref[:, lanes], cosine, sine).astype(bf16)
        v = v_ref[:, lanes]
        ks = [turned(halo_ref[0, :, lanes], pcos, psin).astype(bf16), k[:HALF], k[HALF:]]
        vs = [halo_ref[1, :, lanes], v[:HALF], v[HALF:]]
        parts = []
        for b in range(2):
            result, logs = attend(
                q[b * HALF : (b + 1) * HALF], ks[b], ks[b + 1], vs[b], vs[b + 1], bias if b == 0 else None
            )
            out_ref[b * HALF : (b + 1) * HALF, lanes] = result
            parts.append(wide(logs))
        held = jnp.where(lane == h, jnp.concatenate(parts, axis=0), held)
    log_ref[...] = held


def near_attention(device, cosine, sine, pcos, psin, queries, keys, values, halo):
    vmem = pl.BlockSpec(memory_space=pltpu.VMEM)
    group0 = pl.BlockSpec((None, TOKENS, LOCAL * HEAD), lambda i: (0, 0, 0))
    full = lambda *shape: pl.BlockSpec(shape, lambda i: (0,) * len(shape))
    return pl.pallas_call(
        near_kernel,
        grid=(1,),
        in_specs=[
            pl.BlockSpec(memory_space=pltpu.SMEM),
            full(TOKENS, HEAD // 2),
            full(TOKENS, HEAD // 2),
            full(HALF, HEAD // 2),
            full(HALF, HEAD // 2),
            group0,
            group0,
            group0,
            full(2, HALF, LOCAL * HEAD),
        ],
        out_specs=[full(TOKENS, LOCAL * HEAD), full(TOKENS, HEAD)],
        out_shape=[
            jax.ShapeDtypeStruct((TOKENS, LOCAL * HEAD), f32),
            jax.ShapeDtypeStruct((TOKENS, HEAD), f32),
        ],
        cost_estimate=pl.CostEstimate(flops=16 * 4 * 128 * 256 * 128, bytes_accessed=4 * 2**20, transcendentals=2**19),
        name="near_attention",
    )(device, cosine, sine, pcos, psin, queries, keys, values, halo)


def merge_kernel(x_ref, near_ref, log_ref, far_ref, own_ref, one_ref, two_ref, three_ref, out_ref, far, far_log, mid, mid_log, row_ref):
    x = x_ref[0]
    for steps, ref in enumerate((own_ref, one_ref, two_ref, three_ref)):
        row_ref[lax.rem(x + ROW - steps, ROW)] = ref[...]
    for h in range(LOCAL):
        lanes = slice(h * HEAD, (h + 1) * HEAD)
        for p in range(2):
            piece = 2 * h + p
            logs = rows_to_column(far_ref[piece, HALF : HALF + 1, :], far_ref[piece, HALF + 1 : HALF + 2, :])
            for r in range(8):
                target = pl.ds(p + 2 * r, 16, stride=16)
                far[h % 2, target, :] = far_ref[piece, r * 16 : (r + 1) * 16, :].astype(f32)
                far_log[h % 2, target, :] = logs[r * 16 : (r + 1) * 16]
        chip, head = h // ROW_HEADS, h % ROW_HEADS
        for r in range(4):
            target = pl.ds(r, 64, stride=4)
            rows = TOKENS + 2 * r
            logs = rows_to_column(row_ref[chip, head, rows : rows + 1, :], row_ref[chip, head, rows + 1 : rows + 2, :])
            mid[h % 2, target, :] = row_ref[chip, head, r * 64 : (r + 1) * 64, :].astype(f32)
            mid_log[h % 2, target, :] = logs[:64]
        logs = [wide(log_ref[:, h : h + 1]), mid_log[h % 2], far_log[h % 2]]
        top = jnp.maximum(jnp.maximum(logs[0], logs[1]), logs[2])
        e = [jnp.exp(x - top) for x in logs]
        total = e[0] * near_ref[:, lanes] + e[1] * mid[h % 2] + e[2] * far[h % 2]
        out_ref[:, lanes] = (total / (e[0] + e[1] + e[2])).astype(bf16)


def merge_groups(x, near, log, far, own, others):
    vmem = pl.BlockSpec(memory_space=pltpu.VMEM)
    return pl.pallas_call(
        merge_kernel,
        in_specs=[pl.BlockSpec(memory_space=pltpu.SMEM)] + [vmem] * 7,
        out_specs=vmem,
        out_shape=jax.ShapeDtypeStruct((TOKENS, LOCAL * HEAD), bf16),
        scratch_shapes=[pltpu.VMEM((2, TOKENS, HEAD), f32)] * 4 + [pltpu.VMEM((ROW, *own.shape), bf16)],
        compiler_params=pltpu.CompilerParams(vmem_limit_bytes=12 * 2**20),
        cost_estimate=pl.CostEstimate(flops=2**24, bytes_accessed=2**21, transcendentals=2**19),
        name="merge_groups",
    )(x, near, log, far, own, *others)


def project_kernel(core_ref, mine_ref, other_ref, w_ref, out_ref):
    half = LOCAL * HEAD
    core = core_ref[0]
    mine = pl.ds(pl.multiple_of(core * half, half), half)
    other = pl.ds(pl.multiple_of((1 - core) * half, half), half)
    total = jnp.dot(mine_ref[...], w_ref[mine, :], preferred_element_type=f32)
    total += jnp.dot(other_ref[...], w_ref[other, :], preferred_element_type=f32)
    out_ref[...] = total.astype(bf16)


def project(core, mine, other, w_out):
    vmem = pl.BlockSpec(memory_space=pltpu.VMEM)
    return pl.pallas_call(
        project_kernel,
        in_specs=[pl.BlockSpec(memory_space=pltpu.SMEM), vmem, vmem, vmem],
        out_specs=vmem,
        out_shape=jax.ShapeDtypeStruct((TOKENS, w_out.shape[1]), bf16),
        compiler_params=pltpu.CompilerParams(vmem_limit_bytes=16 * 2**20),
        cost_estimate=pl.CostEstimate(flops=2**30, bytes_accessed=2**22, transcendentals=0),
        name="project",
    )(core, mine, other, w_out)


def tables(count, start):
    inverse = ROPE_BASE ** (-jnp.arange(0, HEAD, 2, dtype=f32) / HEAD)
    angles = (lax.iota(jnp.int32, count) + start).astype(f32)[:, None] * inverse[None, :]
    return jnp.cos(angles), jnp.sin(angles)


def shards(queries, keys, values, w_out):
    devices = lax.axis_size("sp")
    assert queries.shape == (3, TOKENS, LOCAL * HEAD) and devices % PLANE == 0
    planes = [[p * PLANE + i for i in range(PLANE)] for p in range(devices // PLANE)]
    exchange = functools.partial(
        lax.all_to_all, axis_name="sp", split_axis=0, concat_axis=0, axis_index_groups=planes, tiled=True
    )

    def along_row(block, steps):
        return lax.ppermute(block, "sp", [(i, i // ROW * ROW + (i + steps) % ROW) for i in range(devices)])

    def onward(block, distance):
        return lax.ppermute(block, "sp", [(i, i + distance) for i in range(devices - distance)])

    device = lax.axis_index("sp")
    core = lax.axis_index("tp").reshape(1)
    x = lax.rem(device, ROW).reshape(1)
    start = device * TOKENS
    cosine, sine = tables(TOKENS, start)

    kv2 = prepare(2, "kv", (keys, values), x, cosine, sine)
    kv2 = exchange(kv2)
    own = prepare(1, "kvq", (keys, values, queries), x, cosine, sine)
    others = [along_row(own[steps], steps) for steps in range(1, ROW)]
    q2 = prepare(2, "q", (queries,), x, cosine, sine)
    q2 = exchange(q2)
    halo2 = onward(kv2[PLANE // 2 :], PLANE)
    halo1 = onward(pick_last(x, own, others), ROW)
    edge = onward(jnp.stack([keys[0, HALF:], values[0, HALF:]]), 1)
    pcos, psin = tables(HALF, start - HALF)
    near, log = near_attention(device.reshape(1), cosine, sine, pcos, psin, queries, keys, values, edge)
    far = plane_attention((device // PLANE).reshape(1), kv2, q2, halo2)
    far = exchange(far)
    mine, *sent = row_attention(jnp.stack([x[0], device // ROW]), own, others, halo1)
    back = [along_row(block, steps) for steps, block in enumerate(sent, 1)]
    attended = merge_groups(x, near, log, far, mine, back)
    other = lax.ppermute(attended, "tp", [(0, 1), (1, 0)])
    return project(core, attended, other, w_out)


def solution(mesh):
    return jax.shard_map(
        shards,
        mesh=mesh,
        in_specs=(P(None, "sp", "tp"), P(None, "sp", "tp"), P(None, "sp", "tp"), P(None, "tp")),
        out_specs=P("sp", "tp"),
        check_vma=False,
    )
```

time: 131 us -> 120 us (0.916)
  the two profiles are of different devices: /device:TPU:137 before, /device:TPU:97 now
where the time goes in v1:
time: 120 us; the launch traced here: 119 us
  starting transfers between devices  52.7 us (44%)
  Pallas kernels  35.4 us (30%)
  waiting for transfers between devices  18.3 us (15%)
  local copies, waits for them, and re-layouts  9.97 us (8%)
  other arithmetic  2.94 us (2%)
    ppermute x1, starting transfers between devices, shards(): other = lax.ppermute(attended, 'tp', [(0, 1), (1, 0)])  16.3 us
    pallas_call x3, Pallas kernels, prepare(): pl.pallas_call(functools.partial(prepare_kernel, group, kinds), grid_spec...  13 us
    ppermute x3, waiting for transfers between devices, onward(): lax.ppermute(block, 'sp', [(i, i + distance) for i in range(devices - dis...  12.5 us
    ppermute x3, starting transfers between devices, onward(): lax.ppermute(block, 'sp', [(i, i + distance) for i in range(devices - dis...  11.1 us
    pallas_call x1, Pallas kernels, row_attention(): pl.pallas_call(row_kernel, grid=(1,), in_specs=[pl.BlockSpec(memory_space...  8.29 us
    ppermute x6, starting transfers between devices, along_row(): lax.ppermute(block, 'sp', [(i, i // ROW * ROW + (i + steps) % ROW) for i...  7.61 us
    all_to_all x1, starting transfers between devices, shards(): kv2 = exchange(kv2)  6.76 us
    all_to_all x1, starting transfers between devices, shards(): far = exchange(far)  6.75 us
  transfers between devices with their start and end apart: 13, of which 3 were waited for; matrix products, arithmetic and copies ran while one was open for 5% of the time, Pallas kernels for 23%

profile of v1, /device:TPU:97, one launch (start us, length us, event | category | flops | bytes accessed | tf_op | source)
XLA Modules:
  0.0 119.5 jit_solution(1959901337669362743)
XLA Ops:
  0.0 1.3 %multiply_sine_fusion = (f32[256,64]{1,0:T(8,128)}, f32[256,64]{1,0:T(8,128)}) fusion(f32[64]{0:T(128)S(1)} %multiply_power_fusion, f32[256]{0:T(256)S(1)} %add_convert_fusion), kind=kLoop, calls=%fused_computation.4 | loop fusion | flops 16384 | bytes 132352 | tf_op jit(solution)/shard_map/sin | solution.py:391
  1.3 4.3 %shard_map.46 = bf16[16,2,128,128]{3,2,1,0:T(8,128)(2,1)} custom-call(s32[1]{0:T(128)} %bitcast.1.me_ref.x_ref, f32[256,64]{1,0:T(8,128)} %get-tuple-element.21.cos_ref.refs_0_, f32[256,64]{1,0:T(8,128)} %get-tuple-element.20.sin_ref.refs_1_, bf16[3,256,1024]{2,1,0:T(8,128)(2,1)} %refs_2_.5, bf16[3,256,1024]{2,1,0:T(8,128)(2,1)} %refs_3_.3), custom_call_target="tpu_custom_call" | custom-call | flops 1073741824 | bytes 2097152 | tf_op jit(solution)/shard_map/pallas_call | solution.py:97
  5.6 6.8 %all-to-all-start = ((bf16[16,2,128,128]{3,2,1,0:T(8,128)(2,1)}), bf16[16,2,128,128]{3,2,1,0:T(8,128)(2,1)S(1)}, u32[]{:S(2)}, u32[]{:S(2)}) async-start(bf16[16,2,128,128]{3,2,1,0:T(8,128)(2,1)} %shard_map.46), calls=%async_computation | async-start | bytes 2097152 | tf_op jit(solution)/shard_map/all_to_all | solution.py:415
  12.3 4.7 %shard_map.48.own_ref = bf16[4,3,2,256,128]{4,3,2,1,0:T(8,128)(2,1)} custom-call(s32[1]{0:T(128)} %bitcast.1.me_ref.x_ref, f32[256,64]{1,0:T(8,128)} %get-tuple-element.21.cos_ref.refs_0_, f32[256,64]{1,0:T(8,128)} %get-tuple-element.20.sin_ref.refs_1_, bf16[3,256,1024]{2,1,0:T(8,128)(2,1)} %refs_2_.5, bf16[3,256,1024]{2,1,0:T(8,128)(2,1)} %refs_3_.3, ...), custom_call_target="tpu_custom_call" | custom-call | flops 1610612736 | bytes 3145728 | tf_op jit(solution)/shard_map/pallas_call | solution.py:97
  17.1 2.1 %slice_bitcast_fusion = (bf16[3,2,256,128]{3,2,1,0:T(8,128)(2,1)S(1)}, bf16[3,2,256,128]{3,2,1,0:T(8,128)(2,1)S(1)}, bf16[3,2,256,128]{3,2,1,0:T(8,128)(2,1)}) fusion(bf16[4,3,2,256,128]{4,3,2,1,0:T(8,128)(2,1)} %shard_map.48.own_ref), kind=kLoop, calls=%fused_computation.1 | loop fusion | bytes 2359296 | tf_op jit(solution)/shard_map/squeeze | solution.py:417
  19.1 1.4 %collective-permute-start.2 = (bf16[3,2,256,128]{3,2,1,0:T(8,128)(2,1)}, bf16[3,2,256,128]{3,2,1,0:T(8,128)(2,1)}, u32[]{:S(2)}, u32[]{:S(2)}) collective-permute-start(bf16[3,2,256,128]{3,2,1,0:T(8,128)(2,1)} %get-tuple-element.19), channel_id=1, source_target_pairs={{0,2},{2,4},{4,6},{6,0},{8,10},{10,12},{12,14},{14,8},{16,18},{18,... | collective-permute-start | bytes 1179656 | tf_op jit(solution)/shard_map/ppermute | solution.py:403
  20.5 2.4 %collective-permute-start.3 = (bf16[3,2,256,128]{3,2,1,0:T(8,128)(2,1)S(1)}, bf16[3,2,256,128]{3,2,1,0:T(8,128)(2,1)}, u32[]{:S(2)}, u32[]{:S(2)}) collective-permute-start(bf16[3,2,256,128]{3,2,1,0:T(8,128)(2,1)S(1)} %get-tuple-element.18), channel_id=1, source_target_pairs={{0,4},{2,6},{4,0},{6,2},{8,12},{10,14},{12,8},{14,10},{16,20},{18,... | collective-permute-start | bytes 1179656 | tf_op jit(solution)/shard_map/ppermute | solution.py:403
  22.9 1.2 %collective-permute-start.4 = (bf16[3,2,256,128]{3,2,1,0:T(8,128)(2,1)S(1)}, bf16[3,2,256,128]{3,2,1,0:T(8,128)(2,1)}, u32[]{:S(2)}, u32[]{:S(2)}) collective-permute-start(bf16[3,2,256,128]{3,2,1,0:T(8,128)(2,1)S(1)} %get-tuple-element.17), channel_id=1, source_target_pairs={{0,6},{2,0},{4,2},{6,4},{8,14},{10,8},{12,10},{14,12},{16,22},{18,... | collective-permute-start | bytes 1179656 | tf_op jit(solution)/shard_map/ppermute | solution.py:403
  24.1 4.3 %all-to-all-done.kv_ref = bf16[16,2,128,128]{3,2,1,0:T(8,128)(2,1)S(1)} async-done(((bf16[16,2,128,128]{3,2,1,0:T(8,128)(2,1)}), bf16[16,2,128,128]{3,2,1,0:T(8,128)(2,1)S(1)}, u32[]{:S(2)}, u32[]{:S(2)}) %all-to-all-start) | async-done | bytes 1048608 | tf_op jit(solution)/shard_map/all_to_all | solution.py:415
  28.4 0.8 slice.24
  29.2 4.7 %collective-permute-start.1 = (bf16[8,2,128,128]{3,2,1,0:T(8,128)(2,1)}, bf16[8,2,128,128]{3,2,1,0:T(8,128)(2,1)S(1)}, u32[]{:S(2)}, u32[]{:S(2)}) collective-permute-start(bf16[8,2,128,128]{3,2,1,0:T(8,128)(2,1)} %slice.24), channel_id=1, source_target_pairs={{0,32},{2,34},{4,36},{6,38},{8,40},{10,42},{12,44},{14,46},{16,48}... | collective-permute-start | bytes 1572872 | tf_op jit(solution)/shard_map/ppermute | solution.py:406
  33.9 4.0 %shard_map.47 = bf16[16,1,128,128]{3,2,1,0:T(8,128)(2,1)} custom-call(s32[1]{0:T(128)} %bitcast.1.me_ref.x_ref, f32[256,64]{1,0:T(8,128)} %get-tuple-element.21.cos_ref.refs_0_, f32[256,64]{1,0:T(8,128)} %get-tuple-element.20.sin_ref.refs_1_, bf16[3,256,1024]{2,1,0:T(8,128)(2,1)} %refs_4_.1), custom_call_target="tpu_custom_call" | custom-call | flops 536870912 | bytes 1048576 | tf_op jit(solution)/shard_map/pallas_call | solution.py:97
  37.9 4.2 %all-to-all-start.1 = ((bf16[16,1,128,128]{3,2,1,0:T(8,128)(2,1)}), bf16[16,1,128,128]{3,2,1,0:T(8,128)(2,1)S(1)}, u32[]{:S(2)}, u32[]{:S(2)}) async-start(bf16[16,1,128,128]{3,2,1,0:T(8,128)(2,1)} %shard_map.47), calls=%async_computation.1 | async-start | bytes 1048576 | tf_op jit(solution)/shard_map/all_to_all | solution.py:419
  42.1 1.0 slice.18
  43.1 1.0 slice.19
  44.1 0.0 collective-permute-done.2.one_ref
  44.1 0.0 collective-permute-done.3.two_ref
  44.1 0.0 collective-permute-done.4.three_ref
  44.1 2.2 %pick_last.1 = bf16[2,2,2,256,128]{4,3,2,1,0:T(8,128)(2,1)} custom-call(s32[1]{0:T(128)} %bitcast.1.me_ref.x_ref, bf16[4,3,2,256,128]{4,3,2,1,0:T(8,128)(2,1)} %shard_map.48.own_ref, bf16[3,2,256,128]{3,2,1,0:T(8,128)(2,1)} %collective-permute-done.2.one_ref, bf16[3,2,256,128]{3,2,1,0:T(8,128)(2,1)} %collective-permute-done.3.two_ref, ...), custom_call_target="tpu_custom_call" | custom-call | flops 1048576 | bytes 2097152 | tf_op jit(solution)/shard_map/pick_last/pallas_call | solution.py:209
  46.3 3.3 %collective-permute-start.5 = (bf16[2,2,2,256,128]{4,3,2,1,0:T(8,128)(2,1)}, bf16[2,2,2,256,128]{4,3,2,1,0:T(8,128)(2,1)}, u32[]{:S(2)}, u32[]{:S(2)}) collective-permute-start(bf16[2,2,2,256,128]{4,3,2,1,0:T(8,128)(2,1)} %pick_last.1), channel_id=1, source_target_pairs={{0,8},{2,10},{4,12},{6,14},{8,16},{10,18},{12,20},{14,22},{16,24},... | collective-permute-start | bytes 1572872 | tf_op jit(solution)/shard_map/ppermute | solution.py:406
  49.6 0.1 pad_maximum_fusion
  49.6 3.1 %collective-permute-start = (bf16[2,128,1024]{2,1,0:T(8,128)(2,1)S(1)}, bf16[2,128,1024]{2,1,0:T(8,128)(2,1)S(1)}, u32[]{:S(2)}, u32[]{:S(2)}) collective-permute-start(bf16[2,128,1024]{2,1,0:T(8,128)(2,1)S(1)} %pad_maximum_fusion), channel_id=1, source_target_pairs={{0,2},{2,4},{4,6},{6,8},{8,10},{10,12},{12,14},{14,16},{16,18},{18... | collective-permute-start | bytes 1572872 | tf_op jit(solution)/shard_map/ppermute | solution.py:406
  52.8 0.7 pad_add_fusion.x_ref
  53.4 0.0 all-to-all-done.1.q_ref
  53.4 0.0 collective-permute-done.1.halo_ref
  53.4 2.5 %plane_attention.1 = bf16[16,144,128]{2,1,0:T(8,128)(2,1)} custom-call(s32[1]{0:T(128)} %bitcast.3.z_ref, bf16[16,2,128,128]{3,2,1,0:T(8,128)(2,1)S(1)} %all-to-all-done.kv_ref, bf16[16,1,128,128]{3,2,1,0:T(8,128)(2,1)S(1)} %all-to-all-done.1.q_ref, bf16[8,2,128,128]{3,2,1,0:T(8,128)(2,1)S(1)} %collective-permute-done.1.halo_ref), custom_call_target="tpu_custom_call" | custom-call | flops 2147483648 | bytes 3145728 | tf_op jit(solution)/shard_map/plane_attention/pallas_call | solution.py:179
  55.9 6.8 %all-to-all-start.2 = ((bf16[16,144,128]{2,1,0:T(8,128)(2,1)}), bf16[16,144,128]{2,1,0:T(8,128)(2,1)S(1)}, u32[]{:S(2)}, u32[]{:S(2)}) async-start(bf16[16,144,128]{2,1,0:T(8,128)(2,1)} %plane_attention.1), calls=%async_computation.2 | async-start | bytes 1179648 | tf_op jit(solution)/shard_map/all_to_all | solution.py:426
  62.7 12.4 %collective-permute-done.5.halo_ref = bf16[2,2,2,256,128]{4,3,2,1,0:T(8,128)(2,1)} collective-permute-done((bf16[2,2,2,256,128]{4,3,2,1,0:T(8,128)(2,1)}, bf16[2,2,2,256,128]{4,3,2,1,0:T(8,128)(2,1)}, u32[]{:S(2)}, u32[]{:S(2)}) %collective-permute-start.5) | collective-permute-done | bytes 524320 | tf_op jit(solution)/shard_map/ppermute | solution.py:406
  75.2 8.3 %row_attention.1 = (bf16[2,272,128]{2,1,0:T(8,128)(2,1)}, bf16[2,272,128]{2,1,0:T(8,128)(2,1)}, bf16[2,272,128]{2,1,0:T(8,128)(2,1)}, bf16[2,272,128]{2,1,0:T(8,128)(2,1)}) custom-call(s32[2]{0:T(128)} %pad_add_fusion.x_ref, bf16[4,3,2,256,128]{4,3,2,1,0:T(8,128)(2,1)} %shard_map.48.own_ref, bf16[3,2,256,128]{3,2,1,0:T(8,128)(2,1)} %collective-permute-done.2.one_ref, ...), custom_call_target="tpu_custom_call" | custom-call | flops 2147483648 | bytes 3145728 | tf_op jit(solution)/shard_map/row_attention/pallas_call | solution.py:254
  83.4 0.0 collective-permute-start.6
  83.4 0.0 collective-permute-start.7
  83.5 2.6 %collective-permute-start.8 = (bf16[2,272,128]{2,1,0:T(8,128)(2,1)}, bf16[2,272,128]{2,1,0:T(8,128)(2,1)S(1)}, u32[]{:S(2)}, u32[]{:S(2)}) collective-permute-start(bf16[2,272,128]{2,1,0:T(8,128)(2,1)} %get-tuple-element.16), channel_id=1, source_target_pairs={{0,6},{2,0},{4,2},{6,4},{8,14},{10,8},{12,10},{14,12},{16,22},{18,... | collective-permute-start | bytes 417800 | tf_op jit(solution)/shard_map/ppermute | solution.py:403
  86.1 1.0 multiply_sine_fusion.1
  87.1 0.0 collective-permute-done.halo_ref
  87.1 0.0 copy-start.4
  87.1 0.8 copy-done.4
  87.9 0.0 copy-start.2
  87.9 5.5 %near_attention.1 = (f32[256,1024]{1,0:T(8,128)}, f32[256,128]{1,0:T(8,128)}) custom-call(s32[1]{0:T(128)} %bitcast.2.z_ref, f32[256,64]{1,0:T(8,128)} %get-tuple-element.21.cos_ref.refs_0_, f32[256,64]{1,0:T(8,128)} %get-tuple-element.20.sin_ref.refs_1_, f32[128,64]{1,0:T(8,128)} %get-tuple-element.23.pcos_ref, f32[128,64]{1,0:T(8,128)} %get-tuple-element.22.psin_ref, ...), custom_call_target="tpu_custom_call" | custom-call | flops 268435456 | bytes 4194304 | tf_op jit(solution)/shard_map/near_attention/pallas_call | solution.py:300
  93.4 0.0 collective-permute-done.6.one_ref
  93.4 0.0 collective-permute-done.7.two_ref
  93.4 0.0 collective-permute-done.8.three_ref
  93.4 0.0 all-to-all-done.2.far_ref
  93.4 0.0 copy-done.2
  93.4 0.0 copy-start.1
  93.4 1.2 %copy-done.1 = f32[256,1024]{1,0:T(8,128)S(1)} copy-done((f32[256,1024]{1,0:T(8,128)S(1)}, f32[256,1024]{1,0:T(8,128)}, u32[]{:S(2)}) %copy-start.1) | copy-done | bytes 1048600
  94.7 0.0 copy-start.3
  94.7 0.9 copy-done.3
  95.6 1.9 %merge_groups.1.mine_ref = bf16[256,1024]{1,0:T(8,128)(2,1)S(1)} custom-call(s32[1]{0:T(128)} %bitcast.1.me_ref.x_ref, f32[256,1024]{1,0:T(8,128)S(1)} %copy-done.1, f32[256,128]{1,0:T(8,128)S(1)} %copy-done.3, bf16[16,144,128]{2,1,0:T(8,128)(2,1)S(1)} %all-to-all-done.2.far_ref, bf16[2,272,128]{2,1,0:T(8,128)(2,1)S(1)} %copy-done.2, ...), custom_call_target="tpu_custom_call" | custom-call | flops 16777216 | bytes 2097152 | tf_op jit(solution)/shard_map/merge_groups/pallas_call | solution.py:353
  97.4 16.3 %collective-permute-start.9 = (bf16[256,1024]{1,0:T(8,128)(2,1)S(1)}, bf16[256,1024]{1,0:T(8,128)(2,1)S(1)}, u32[]{:S(2)}, u32[]{:S(2)}) collective-permute-start(bf16[256,1024]{1,0:T(8,128)(2,1)S(1)} %merge_groups.1.mine_ref), channel_id=1, source_target_pairs={{0,1},{1,0},{2,3},{3,2},{4,5},{5,4},{6,7},{7,6},{8,9},{9,8},{10,11... | collective-permute-start | bytes 1572872 | tf_op jit(solution)/shard_map/ppermute | solution.py:430
  113.7 1.5 %collective-permute-done.9.other_ref = bf16[256,1024]{1,0:T(8,128)(2,1)S(1)} collective-permute-done((bf16[256,1024]{1,0:T(8,128)(2,1)S(1)}, bf16[256,1024]{1,0:T(8,128)(2,1)S(1)}, u32[]{:S(2)}, u32[]{:S(2)}) %collective-permute-start.9) | collective-permute-done | bytes 524320 | tf_op jit(solution)/shard_map/ppermute | solution.py:430
  115.2 0.0 copy-start
  115.2 2.2 %copy-done = bf16[2048,1024]{1,0:T(8,128)(2,1)S(1)} copy-done((bf16[2048,1024]{1,0:T(8,128)(2,1)S(1)}, bf16[2048,1024]{1,0:T(8,128)(2,1)}, u32[]{:S(2)}) %copy-start) | copy-done | bytes 4194328
  117.4 2.0 %project.1 = bf16[256,1024]{1,0:T(8,128)(2,1)} custom-call(s32[1]{0:T(128)} %bitcast.core_ref, bf16[256,1024]{1,0:T(8,128)(2,1)S(1)} %merge_groups.1.mine_ref, bf16[256,1024]{1,0:T(8,128)(2,1)S(1)} %collective-permute-done.9.other_ref, bf16[2048,1024]{1,0:T(8,128)(2,1)S(1)} %copy-done), custom_call_target="tpu_custom_call" | custom-call | flops 1073741824 | bytes 4194304 | tf_op jit(solution)/shard_map/project/pallas_call | solution.py:377
  (3 shorter events, 0.0 us)
Async XLA Ops:
  5.6 22.8 %all-to-all-start = ((bf16[16,2,128,128]{3,2,1,0:T(8,128)(2,1)}), bf16[16,2,128,128]{3,2,1,0:T(8,128)(2,1)S(1)}, u32[]{:S(2)}, u32[]{:S(2)}) async-start(bf16[16,2,128,128]{3,2,1,0:T(8,128)(2,1)} %shard_map.46), calls=%async_computation | async-start | bytes 2097152 | tf_op jit(solution)/shard_map/all_to_all | solution.py:415
  19.1 24.9 %collective-permute-start.2 = (bf16[3,2,256,128]{3,2,1,0:T(8,128)(2,1)}, bf16[3,2,256,128]{3,2,1,0:T(8,128)(2,1)}, u32[]{:S(2)}, u32[]{:S(2)}) collective-permute-start(bf16[3,2,256,128]{3,2,1,0:T(8,128)(2,1)} %get-tuple-element.19), channel_id=1, source_target_pairs={{0,2},{2,4},{4,6},{6,0},{8,10},{10,12},{12,14},{14,8},{16,18},{18,... | collective-permute-start | bytes 1179656 | tf_op jit(solution)/shard_map/ppermute | solution.py:403
  20.5 23.6 %collective-permute-start.3 = (bf16[3,2,256,128]{3,2,1,0:T(8,128)(2,1)S(1)}, bf16[3,2,256,128]{3,2,1,0:T(8,128)(2,1)}, u32[]{:S(2)}, u32[]{:S(2)}) collective-permute-start(bf16[3,2,256,128]{3,2,1,0:T(8,128)(2,1)S(1)} %get-tuple-element.18), channel_id=1, source_target_pairs={{0,4},{2,6},{4,0},{6,2},{8,12},{10,14},{12,8},{14,10},{16,20},{18,... | collective-permute-start | bytes 1179656 | tf_op jit(solution)/shard_map/ppermute | solution.py:403
  22.9 21.2 %collective-permute-start.4 = (bf16[3,2,256,128]{3,2,1,0:T(8,128)(2,1)S(1)}, bf16[3,2,256,128]{3,2,1,0:T(8,128)(2,1)}, u32[]{:S(2)}, u32[]{:S(2)}) collective-permute-start(bf16[3,2,256,128]{3,2,1,0:T(8,128)(2,1)S(1)} %get-tuple-element.17), channel_id=1, source_target_pairs={{0,6},{2,0},{4,2},{6,4},{8,14},{10,8},{12,10},{14,12},{16,22},{18,... | collective-permute-start | bytes 1179656 | tf_op jit(solution)/shard_map/ppermute | solution.py:403
  29.2 24.2 %collective-permute-start.1 = (bf16[8,2,128,128]{3,2,1,0:T(8,128)(2,1)}, bf16[8,2,128,128]{3,2,1,0:T(8,128)(2,1)S(1)}, u32[]{:S(2)}, u32[]{:S(2)}) collective-permute-start(bf16[8,2,128,128]{3,2,1,0:T(8,128)(2,1)} %slice.24), channel_id=1, source_target_pairs={{0,32},{2,34},{4,36},{6,38},{8,40},{10,42},{12,44},{14,46},{16,48}... | collective-permute-start | bytes 1572872 | tf_op jit(solution)/shard_map/ppermute | solution.py:406
  37.9 15.5 %all-to-all-start.1 = ((bf16[16,1,128,128]{3,2,1,0:T(8,128)(2,1)}), bf16[16,1,128,128]{3,2,1,0:T(8,128)(2,1)S(1)}, u32[]{:S(2)}, u32[]{:S(2)}) async-start(bf16[16,1,128,128]{3,2,1,0:T(8,128)(2,1)} %shard_map.47), calls=%async_computation.1 | async-start | bytes 1048576 | tf_op jit(solution)/shard_map/all_to_all | solution.py:419
  46.3 28.8 %collective-permute-start.5 = (bf16[2,2,2,256,128]{4,3,2,1,0:T(8,128)(2,1)}, bf16[2,2,2,256,128]{4,3,2,1,0:T(8,128)(2,1)}, u32[]{:S(2)}, u32[]{:S(2)}) collective-permute-start(bf16[2,2,2,256,128]{4,3,2,1,0:T(8,128)(2,1)} %pick_last.1), channel_id=1, source_target_pairs={{0,8},{2,10},{4,12},{6,14},{8,16},{10,18},{12,20},{14,22},{16,24},... | collective-permute-start | bytes 1572872 | tf_op jit(solution)/shard_map/ppermute | solution.py:406
  49.6 37.4 %collective-permute-start = (bf16[2,128,1024]{2,1,0:T(8,128)(2,1)S(1)}, bf16[2,128,1024]{2,1,0:T(8,128)(2,1)S(1)}, u32[]{:S(2)}, u32[]{:S(2)}) collective-permute-start(bf16[2,128,1024]{2,1,0:T(8,128)(2,1)S(1)} %pad_maximum_fusion), channel_id=1, source_target_pairs={{0,2},{2,4},{4,6},{6,8},{8,10},{10,12},{12,14},{14,16},{16,18},{18... | collective-permute-start | bytes 1572872 | tf_op jit(solution)/shard_map/ppermute | solution.py:406
  55.9 37.5 %all-to-all-start.2 = ((bf16[16,144,128]{2,1,0:T(8,128)(2,1)}), bf16[16,144,128]{2,1,0:T(8,128)(2,1)S(1)}, u32[]{:S(2)}, u32[]{:S(2)}) async-start(bf16[16,144,128]{2,1,0:T(8,128)(2,1)} %plane_attention.1), calls=%async_computation.2 | async-start | bytes 1179648 | tf_op jit(solution)/shard_map/all_to_all | solution.py:426
  83.4 9.9 %collective-permute-start.6 = (bf16[2,272,128]{2,1,0:T(8,128)(2,1)}, bf16[2,272,128]{2,1,0:T(8,128)(2,1)S(1)}, u32[]{:S(2)}, u32[]{:S(2)}) collective-permute-start(bf16[2,272,128]{2,1,0:T(8,128)(2,1)} %get-tuple-element.14), channel_id=1, source_target_pairs={{0,2},{2,4},{4,6},{6,0},{8,10},{10,12},{12,14},{14,8},{16,18},{18,... | collective-permute-start | bytes 417800 | tf_op jit(solution)/shard_map/ppermute | solution.py:403
  83.4 9.9 %collective-permute-start.7 = (bf16[2,272,128]{2,1,0:T(8,128)(2,1)}, bf16[2,272,128]{2,1,0:T(8,128)(2,1)S(1)}, u32[]{:S(2)}, u32[]{:S(2)}) collective-permute-start(bf16[2,272,128]{2,1,0:T(8,128)(2,1)} %get-tuple-element.15), channel_id=1, source_target_pairs={{0,4},{2,6},{4,0},{6,2},{8,12},{10,14},{12,8},{14,10},{16,20},{18,... | collective-permute-start | bytes 417800 | tf_op jit(solution)/shard_map/ppermute | solution.py:403
  83.5 9.9 %collective-permute-start.8 = (bf16[2,272,128]{2,1,0:T(8,128)(2,1)}, bf16[2,272,128]{2,1,0:T(8,128)(2,1)S(1)}, u32[]{:S(2)}, u32[]{:S(2)}) collective-permute-start(bf16[2,272,128]{2,1,0:T(8,128)(2,1)} %get-tuple-element.16), channel_id=1, source_target_pairs={{0,6},{2,0},{4,2},{6,4},{8,14},{10,8},{12,10},{14,12},{16,22},{18,... | collective-permute-start | bytes 417800 | tf_op jit(solution)/shard_map/ppermute | solution.py:403
  87.1 0.8 copy-start.4
  87.9 5.5 %copy-start.2 = (bf16[2,272,128]{2,1,0:T(8,128)(2,1)S(1)}, bf16[2,272,128]{2,1,0:T(8,128)(2,1)}, u32[]{:S(2)}) copy-start(bf16[2,272,128]{2,1,0:T(8,128)(2,1)} %get-tuple-element.13.own_ref) | copy-start | bytes 417796
  93.4 1.2 %copy-start.1 = (f32[256,1024]{1,0:T(8,128)S(1)}, f32[256,1024]{1,0:T(8,128)}, u32[]{:S(2)}) copy-start(f32[256,1024]{1,0:T(8,128)} %get-tuple-element.11.near_ref) | copy-start | bytes 3145732
  94.7 0.9 copy-start.3
  97.4 17.8 %collective-permute-start.9 = (bf16[256,1024]{1,0:T(8,128)(2,1)S(1)}, bf16[256,1024]{1,0:T(8,128)(2,1)S(1)}, u32[]{:S(2)}, u32[]{:S(2)}) collective-permute-start(bf16[256,1024]{1,0:T(8,128)(2,1)S(1)} %merge_groups.1.mine_ref), channel_id=1, source_target_pairs={{0,1},{1,0},{2,3},{3,2},{4,5},{5,4},{6,7},{7,6},{8,9},{9,8},{10,11... | collective-permute-start | bytes 1572872 | tf_op jit(solution)/shard_map/ppermute | solution.py:430
  115.2 2.2 %copy-start = (bf16[2048,1024]{1,0:T(8,128)(2,1)S(1)}, bf16[2048,1024]{1,0:T(8,128)(2,1)}, u32[]{:S(2)}) copy-start(bf16[2048,1024]{1,0:T(8,128)(2,1)} %w_ref.1) | copy-start | bytes 12582916

commit v2 on v1

--- a/solution.py
+++ b/solution.py
@@ -47,68 +47,82 @@
     row = iota((TOKENS, TOKENS), 0)
     token = iota((TOKENS, TOKENS), 1)
     stride = STRIDES[group]
-    steps = TOKENS // stride
+    shift = (TOKENS // stride).bit_length() - 1
+    step = row & (2**shift - 1)
     if group == 2:
-        within = row % HALF
-        picked = row // HALF + 2 * (within // steps) + stride * (within % steps)
+        picked = (row >> 7) + 2 * ((row & (HALF - 1)) >> shift) + stride * step
     else:
-        picked = row // steps + stride * (row % steps)
+        picked = (row >> shift) + stride * step
     return jnp.where(picked == token, 1.0, 0.0).astype(bf16)
 
 
-def prepare_kernel(group, kinds, me_ref, *refs):
-    cos_ref, sin_ref = refs[:2]
-    ins, out_ref, sort_ref, full_ref = refs[2:-3], refs[-3], refs[-2], refs[-1]
-
+def load_kind(kind, x, cosine, sine):
+    if kind == "v":
+        return x
+    heads = [turned(x[:, h * HEAD : (h + 1) * HEAD], cosine, sine) for h in range(2)]
+    if kind == "q":
+        heads = [x * SCALE for x in heads]
+    return jnp.concatenate([x.astype(bf16) for x in heads], axis=1)
+
+
+def plane_pieces_kernel(cos_ref, sin_ref, k_ref, v_ref, q_ref, out_ref, sort_ref, full_ref):
     @pl.when(pl.program_id(0) == 0)
     def _():
-        sort_ref[...] = sorting(group)
+        sort_ref[...] = sorting(2)
         full_ref[0], full_ref[1] = full_tables(cos_ref, sin_ref)
 
     cosine, sine = full_ref[0], full_ref[1]
-    for a, kind in enumerate(kinds):
-        x = ins[a][...]
-        if kind != "v":
-            heads = [turned(x[:, h * HEAD : (h + 1) * HEAD], cosine, sine) for h in range(2)]
-            if kind == "q":
-                heads = [x * SCALE for x in heads]
-            x = jnp.concatenate([x.astype(bf16) for x in heads], axis=1)
+    for a, (kind, ref) in enumerate((("k", k_ref), ("v", v_ref), ("q", q_ref))):
+        x = load_kind(kind, ref[...], cosine, sine)
         y = jnp.dot(sort_ref[...], x, preferred_element_type=f32).astype(bf16)
         for h in range(2):
-            lanes = slice(h * HEAD, (h + 1) * HEAD)
-            if group == 2:
-                for p in range(2):
-                    out_ref[2 * h + p, a] = y[p * HALF : (p + 1) * HALF, lanes]
-            else:
-                out_ref[a, h] = y[:, lanes]
-
-
-def prepare(group, kinds, arrays, me, cosine, sine):
-    n = len(kinds)
-    table = pl.BlockSpec((TOKENS, HEAD // 2), lambda g, me: (0, 0))
-    if group == 2:
-        out_spec = pl.BlockSpec((4, n, HALF, HEAD), lambda g, me: (g, 0, 0, 0))
-        out_shape = (PLANE, n, HALF, HEAD)
-    else:
-        out_spec = pl.BlockSpec(
-            (None, n, ROW_HEADS, TOKENS, HEAD), lambda g, me: (lax.rem(g + ROW - me[0], ROW), 0, 0, 0, 0)
-        )
-        out_shape = (ROW, n, ROW_HEADS, TOKENS, HEAD)
-    return pl.pallas_call(
-        functools.partial(prepare_kernel, group, kinds),
-        grid_spec=pltpu.PrefetchScalarGridSpec(
-            num_scalar_prefetch=1,
-            grid=(LOCAL // 2,),
-            in_specs=[table, table]
-            + [pl.BlockSpec((None, TOKENS, 2 * HEAD), lambda g, me: (group, 0, g)) for _ in kinds],
-            out_specs=out_spec,
-            scratch_shapes=[pltpu.VMEM((TOKENS, TOKENS), bf16), pltpu.VMEM((2, TOKENS, HEAD), f32)],
-        ),
-        out_shape=jax.ShapeDtypeStruct(out_shape, bf16),
-        cost_estimate=pl.CostEstimate(
-            flops=n * LOCAL * 2 * TOKENS * TOKENS * HEAD * 4, bytes_accessed=n * 2**20, transcendentals=0
-        ),
-    )(me, cosine, sine, *arrays)
+            for p in range(2):
+                out_ref[2 * h + p, a] = y[p * HALF : (p + 1) * HALF, h * HEAD : (h + 1) * HEAD]
+
+
+def plane_pieces(keys, values, queries, cosine, sine):
+    table = pl.BlockSpec((TOKENS, HEAD // 2), lambda g: (0, 0))
+    return pl.pallas_call(
+        plane_pieces_kernel,
+        grid=(LOCAL // 2,),
+        in_specs=[table, table] + [pl.BlockSpec((None, TOKENS, 2 * HEAD), lambda g: (2, 0, g))] * 3,
+        out_specs=pl.BlockSpec((4, 3, HALF, HEAD), lambda g: (g, 0, 0, 0)),
+        scratch_shapes=[pltpu.VMEM((TOKENS, TOKENS), bf16), pltpu.VMEM((2, TOKENS, HEAD), f32)],
+        out_shape=jax.ShapeDtypeStruct((PLANE, 3, HALF, HEAD), bf16),
+        cost_estimate=pl.CostEstimate(flops=2**30, bytes_accessed=3 * 2**20, transcendentals=0),
+        name="plane_pieces",
+    )(cosine, sine, keys, values, queries)
+
+
+def row_pieces_kernel(x_ref, cos_ref, sin_ref, k_ref, v_ref, q_ref, *refs):
+    outs, in_ref, sem = refs[:ROW], refs[ROW], refs[ROW + 1]
+    copies = [pltpu.make_async_copy(ref.at[1], in_ref.at[a], sem.at[a]) for a, ref in enumerate((k_ref, v_ref, q_ref))]
+    for copy in copies:
+        copy.start()
+    sort = sorting(1)
+    cosine, sine = full_tables(cos_ref, sin_ref)
+    width = ROW_HEADS * HEAD
+    for a, kind in enumerate("kvq"):
+        copies[a].wait()
+        for steps in range(ROW):
+            chip = lax.rem(x_ref[0] + steps, ROW)
+            x = in_ref[a, :, pl.ds(pl.multiple_of(chip * width, width), width)]
+            y = jnp.dot(sort, load_kind(kind, x, cosine, sine), preferred_element_type=f32).astype(bf16)
+            for h in range(ROW_HEADS):
+                outs[steps][a, h] = y[:, h * HEAD : (h + 1) * HEAD]
+
+
+def row_pieces(x, keys, values, queries, cosine, sine):
+    vmem, hbm = pl.BlockSpec(memory_space=pltpu.VMEM), pl.BlockSpec(memory_space=pltpu.HBM)
+    return pl.pallas_call(
+        row_pieces_kernel,
+        in_specs=[pl.BlockSpec(memory_space=pltpu.SMEM), vmem, vmem, hbm, hbm, hbm],
+        out_specs=[vmem] * ROW,
+        scratch_shapes=[pltpu.VMEM((3, TOKENS, LOCAL * HEAD), bf16), pltpu.SemaphoreType.DMA((3,))],
+        out_shape=[jax.ShapeDtypeStruct((3, ROW_HEADS, TOKENS, HEAD), bf16)] * ROW,
+        cost_estimate=pl.CostEstimate(flops=2**30, bytes_accessed=3 * 2**20, transcendentals=0),
+        name="row_pieces",
+    )(x, cosine, sine, keys, values, queries)
 
 
 def dot_t(a, b):
@@ -155,7 +169,7 @@
     )
 
 
-def plane_kernel(z_ref, kv_ref, q_ref, halo_ref, out_ref, logs_ref):
+def plane_kernel(z_ref, in_ref, halo_ref, out_ref, logs_ref):
     bias = jnp.where(z_ref[0] == 0, MASKED, -MASKED)
     for r in range(8):
         rows = slice(r * 16, (r + 1) * 16)
@@ -163,9 +177,9 @@
         vs = [jnp.concatenate([halo_ref[i, 1, rows, :] for i in range(8)], axis=0)]
         for b in range(2):
             chips = range(8 * b, 8 * b + 8)
-            ks.append(jnp.concatenate([kv_ref[s, 0, rows, :] for s in chips], axis=0))
-            vs.append(jnp.concatenate([kv_ref[s, 1, rows, :] for s in chips], axis=0))
-            q = jnp.concatenate([q_ref[s, 0, rows, :] for s in chips], axis=0)
+            ks.append(jnp.concatenate([in_ref[s, 0, rows, :] for s in chips], axis=0))
+            vs.append(jnp.concatenate([in_ref[s, 1, rows, :] for s in chips], axis=0))
+            q = jnp.concatenate([in_ref[s, 2, rows, :] for s in chips], axis=0)
             result, logs = attend(q, ks[b], ks[b + 1], vs[b], vs[b + 1], bias if b == 0 else None)
             for i, s in enumerate(chips):
                 out_ref[s, rows, :] = result[i * 16 : (i + 1) * 16].astype(bf16)
@@ -174,18 +188,18 @@
         out_ref[s, HALF:, :] = column_to_rows(logs_ref[s]).astype(bf16)
 
 
-def plane_attention(z, kv, q, halo):
+def plane_attention(z, held, halo):
     vmem = pl.BlockSpec(memory_space=pltpu.VMEM)
     return pl.pallas_call(
         plane_kernel,
-        in_specs=[pl.BlockSpec(memory_space=pltpu.SMEM), vmem, vmem, vmem],
+        in_specs=[pl.BlockSpec(memory_space=pltpu.SMEM), vmem, vmem],
         out_specs=vmem,
         out_shape=jax.ShapeDtypeStruct((PLANE, RETURN_ROWS, HEAD), bf16),
         scratch_shapes=[pltpu.VMEM((PLANE, HALF, 1), f32)],
-        compiler_params=pltpu.CompilerParams(vmem_limit_bytes=20 * 2**20),
+        compiler_params=pltpu.CompilerParams(vmem_limit_bytes=8 * 2**20),
         cost_estimate=pl.CostEstimate(flops=2**31, bytes_accessed=3 * 2**20, transcendentals=2**19),
         name="plane_attention",
-    )(z, kv, q, halo)
+    )(z, held, halo)
 
 
 def pick_kernel(x_ref, own_ref, one_ref, two_ref, three_ref, out_ref):
@@ -198,27 +212,21 @@
             out_ref[chip - ROW // 2] = ref[:2]
 
 
-def row_specs(own, others):
-    piece = own.shape[1:]
-    whole = lambda shape: pl.BlockSpec(shape, lambda i: (0,) * len(shape))
-    return [pl.BlockSpec((None, *piece), lambda i: (0,) * (len(piece) + 1))] + [whole(o.shape) for o in others]
-
-
-def pick_last(x, own, others):
-    shape = (2, 2, ROW_HEADS, TOKENS, HEAD)
+def pick_last(x, pieces):
+    vmem = pl.BlockSpec(memory_space=pltpu.VMEM)
     return pl.pallas_call(
         pick_kernel,
-        grid=(1,),
-        in_specs=[pl.BlockSpec(memory_space=pltpu.SMEM)] + row_specs(own, others),
-        out_specs=pl.BlockSpec(shape, lambda i: (0,) * 5),
-        out_shape=jax.ShapeDtypeStruct(shape, bf16),
+        in_specs=[pl.BlockSpec(memory_space=pltpu.SMEM)] + [vmem] * ROW,
+        out_specs=vmem,
+        out_shape=jax.ShapeDtypeStruct((2, 2, ROW_HEADS, TOKENS, HEAD), bf16),
+        compiler_params=pltpu.CompilerParams(vmem_limit_bytes=4 * 2**20),
         cost_estimate=pl.CostEstimate(flops=2**20, bytes_accessed=2**21, transcendentals=0),
         name="pick_last",
-    )(x, own, *others)
+    )(x, *pieces)
 
 
 def row_kernel(x_ref, own_ref, one_ref, two_ref, three_ref, halo_ref, *refs):
-    outs, in_ref, res_ref = refs[:4], refs[4], refs[5]
+    outs, in_ref, res_ref = refs[:4], *refs[4:]
     x = x_ref[0]
     bias = jnp.where(x_ref[1] == 0, MASKED, -MASKED)
     for steps, ref in enumerate((own_ref, one_ref, two_ref, three_ref)):
@@ -249,32 +257,39 @@
         out[...] = res_ref[lax.rem(x + steps, ROW)]
 
 
-def row_attention(place, own, others, halo):
+def row_attention(place, pieces, halo):
     shape = (ROW_HEADS, ROW_RETURN, HEAD)
+    vmem = pl.BlockSpec(memory_space=pltpu.VMEM)
     return pl.pallas_call(
         row_kernel,
-        grid=(1,),
-        in_specs=[pl.BlockSpec(memory_space=pltpu.SMEM)]
-        + row_specs(own, others)
-        + [pl.BlockSpec(halo.shape, lambda i: (0,) * 5)],
-        out_specs=[pl.BlockSpec(shape, lambda i: (0,) * 3)] * ROW,
+        in_specs=[pl.BlockSpec(memory_space=pltpu.SMEM)] + [vmem] * (ROW + 1),
+        out_specs=[vmem] * ROW,
         out_shape=[jax.ShapeDtypeStruct(shape, bf16)] * ROW,
         scratch_shapes=[
             pltpu.VMEM((ROW, 3, ROW_HEADS, TOKENS, HEAD), bf16),
             pltpu.VMEM((ROW, *shape), bf16),
         ],
+        compiler_params=pltpu.CompilerParams(vmem_limit_bytes=10 * 2**20),
         cost_estimate=pl.CostEstimate(flops=2**31, bytes_accessed=3 * 2**20, transcendentals=2**19),
         name="row_attention",
-    )(place, own, *others, halo)
-
-
-def near_kernel(z_ref, cos_ref, sin_ref, pcos_ref, psin_ref, q_ref, k_ref, v_ref, halo_ref, out_ref, log_ref):
+    )(place, *pieces, halo)
+
+
+def near_kernel(
+    z_ref, cos_ref, sin_ref, pcos_ref, psin_ref, q_hbm, k_hbm, v_hbm, halo_ref, out_ref, log_ref, q_ref, k_ref, v_ref, sem
+):
+    pairs = ((q_hbm, q_ref), (k_hbm, k_ref), (v_hbm, v_ref))
+    copies = [pltpu.make_async_copy(a.at[0], b, sem.at[i]) for i, (a, b) in enumerate(pairs)]
+    for copy in copies:
+        copy.start()
     bias = jnp.where(z_ref[0] == 0, MASKED, -MASKED)
     cosine, sine = full_tables(cos_ref, sin_ref)
     pcos, psin = full_tables(pcos_ref, psin_ref)
     lane = iota((TOKENS, HEAD), 1)
 
     held = jnp.zeros((TOKENS, HEAD), f32)
+    for copy in copies:
+        copy.wait()
     for h in range(LOCAL):
         lanes = slice(h * HEAD, (h + 1) * HEAD)
         q = (turned(q_ref[:, lanes], cosine, sine) * SCALE).astype(bf16)
@@ -287,36 +302,24 @@
             result, logs = attend(
                 q[b * HALF : (b + 1) * HALF], ks[b], ks[b + 1], vs[b], vs[b + 1], bias if b == 0 else None
             )
-            out_ref[b * HALF : (b + 1) * HALF, lanes] = result
+            out_ref[b * HALF : (b + 1) * HALF, lanes] = result.astype(bf16)
             parts.append(wide(logs))
         held = jnp.where(lane == h, jnp.concatenate(parts, axis=0), held)
     log_ref[...] = held
 
 
 def near_attention(device, cosine, sine, pcos, psin, queries, keys, values, halo):
-    vmem = pl.BlockSpec(memory_space=pltpu.VMEM)
-    group0 = pl.BlockSpec((None, TOKENS, LOCAL * HEAD), lambda i: (0, 0, 0))
-    full = lambda *shape: pl.BlockSpec(shape, lambda i: (0,) * len(shape))
+    vmem, hbm = pl.BlockSpec(memory_space=pltpu.VMEM), pl.BlockSpec(memory_space=pltpu.HBM)
     return pl.pallas_call(
         near_kernel,
-        grid=(1,),
-        in_specs=[
-            pl.BlockSpec(memory_space=pltpu.SMEM),
-            full(TOKENS, HEAD // 2),
-            full(TOKENS, HEAD // 2),
-            full(HALF, HEAD // 2),
-            full(HALF, HEAD // 2),
-            group0,
-            group0,
-            group0,
-            full(2, HALF, LOCAL * HEAD),
-        ],
-        out_specs=[full(TOKENS, LOCAL * HEAD), full(TOKENS, HEAD)],
+        in_specs=[pl.BlockSpec(memory_space=pltpu.SMEM)] + [vmem] * 4 + [hbm] * 3 + [vmem],
+        out_specs=[vmem] * 2,
         out_shape=[
-            jax.ShapeDtypeStruct((TOKENS, LOCAL * HEAD), f32),
+            jax.ShapeDtypeStruct((TOKENS, LOCAL * HEAD), bf16),
             jax.ShapeDtypeStruct((TOKENS, HEAD), f32),
         ],
-        cost_estimate=pl.CostEstimate(flops=16 * 4 * 128 * 256 * 128, bytes_accessed=4 * 2**20, transcendentals=2**19),
+        scratch_shapes=[pltpu.VMEM((TOKENS, LOCAL * HEAD), bf16)] * 3 + [pltpu.SemaphoreType.DMA((3,))],
+        cost_estimate=pl.CostEstimate(flops=2**31, bytes_accessed=4 * 2**20, transcendentals=2**19),
         name="near_attention",
     )(device, cosine, sine, pcos, psin, queries, keys, values, halo)
 
@@ -344,7 +347,7 @@
         logs = [wide(log_ref[:, h : h + 1]), mid_log[h % 2], far_log[h % 2]]
         top = jnp.maximum(jnp.maximum(logs[0], logs[1]), logs[2])
         e = [jnp.exp(x - top) for x in logs]
-        total = e[0] * near_ref[:, lanes] + e[1] * mid[h % 2] + e[2] * far[h % 2]
+        total = e[0] * near_ref[:, lanes].astype(f32) + e[1] * mid[h % 2] + e[2] * far[h % 2]
         out_ref[:, lanes] = (total / (e[0] + e[1] + e[2])).astype(bf16)
 
 
@@ -356,33 +359,42 @@
         out_specs=vmem,
         out_shape=jax.ShapeDtypeStruct((TOKENS, LOCAL * HEAD), bf16),
         scratch_shapes=[pltpu.VMEM((2, TOKENS, HEAD), f32)] * 4 + [pltpu.VMEM((ROW, *own.shape), bf16)],
-        compiler_params=pltpu.CompilerParams(vmem_limit_bytes=12 * 2**20),
+        compiler_params=pltpu.CompilerParams(vmem_limit_bytes=8 * 2**20),
         cost_estimate=pl.CostEstimate(flops=2**24, bytes_accessed=2**21, transcendentals=2**19),
         name="merge_groups",
     )(x, near, log, far, own, *others)
 
 
-def project_kernel(core_ref, mine_ref, other_ref, w_ref, out_ref):
+def project_kernel(start_ref, in_ref, w_hbm, *refs):
+    *partial, out_ref, w_ref, sem = refs
     half = LOCAL * HEAD
-    core = core_ref[0]
-    mine = pl.ds(pl.multiple_of(core * half, half), half)
-    other = pl.ds(pl.multiple_of((1 - core) * half, half), half)
-    total = jnp.dot(mine_ref[...], w_ref[mine, :], preferred_element_type=f32)
-    total += jnp.dot(other_ref[...], w_ref[other, :], preferred_element_type=f32)
-    out_ref[...] = total.astype(bf16)
-
-
-def project(core, mine, other, w_out):
-    vmem = pl.BlockSpec(memory_space=pltpu.VMEM)
+    chunk = half // 4
+    copies = []
+    for c in range(4):
+        rows = pl.ds(pl.multiple_of(start_ref[0] * half + c * chunk, chunk), chunk)
+        copies.append(pltpu.make_async_copy(w_hbm.at[rows], w_ref.at[pl.ds(c * chunk, chunk)], sem.at[c]))
+        copies[-1].start()
+    total = partial[0][...] if partial else None
+    for c in range(4):
+        copies[c].wait()
+        part = slice(c * chunk, (c + 1) * chunk)
+        term = jnp.dot(in_ref[:, part], w_ref[part, :], preferred_element_type=f32)
+        total = term if total is None else total + term
+    out_ref[...] = total.astype(out_ref.dtype)
+
+
+def project(core, block, w_out, partial, dtype):
+    vmem, hbm = pl.BlockSpec(memory_space=pltpu.VMEM), pl.BlockSpec(memory_space=pltpu.HBM)
     return pl.pallas_call(
         project_kernel,
-        in_specs=[pl.BlockSpec(memory_space=pltpu.SMEM), vmem, vmem, vmem],
+        in_specs=[pl.BlockSpec(memory_space=pltpu.SMEM), vmem, hbm] + [vmem] * len(partial),
         out_specs=vmem,
-        out_shape=jax.ShapeDtypeStruct((TOKENS, w_out.shape[1]), bf16),
-        compiler_params=pltpu.CompilerParams(vmem_limit_bytes=16 * 2**20),
-        cost_estimate=pl.CostEstimate(flops=2**30, bytes_accessed=2**22, transcendentals=0),
+        out_shape=jax.ShapeDtypeStruct((TOKENS, w_out.shape[1]), dtype),
+        scratch_shapes=[pltpu.VMEM((LOCAL * HEAD, w_out.shape[1]), bf16), pltpu.SemaphoreType.DMA((4,))],
+        compiler_params=pltpu.CompilerParams(vmem_limit_bytes=58 * 2**20),
+        cost_estimate=pl.CostEstimate(flops=2**29, bytes_accessed=2**22, transcendentals=0),
         name="project",
-    )(core, mine, other, w_out)
+    )(core, block, w_out, *partial)
 
 
 def tables(count, start):
@@ -411,24 +423,24 @@
     start = device * TOKENS
     cosine, sine = tables(TOKENS, start)
 
-    kv2 = prepare(2, "kv", (keys, values), x, cosine, sine)
-    kv2 = exchange(kv2)
-    own = prepare(1, "kvq", (keys, values, queries), x, cosine, sine)
-    others = [along_row(own[steps], steps) for steps in range(1, ROW)]
-    q2 = prepare(2, "q", (queries,), x, cosine, sine)
-    q2 = exchange(q2)
-    halo2 = onward(kv2[PLANE // 2 :], PLANE)
-    halo1 = onward(pick_last(x, own, others), ROW)
+    held = plane_pieces(keys, values, queries, cosine, sine)
+    held = exchange(held)
+    own, *others = row_pieces(x, keys, values, queries, cosine, sine)
+    pieces = [own] + [along_row(block, steps) for steps, block in enumerate(others, 1)]
     edge = onward(jnp.stack([keys[0, HALF:], values[0, HALF:]]), 1)
+    halo2 = onward(held[PLANE // 2 :, :2], PLANE)
+    last = pick_last(x, pieces)
+    halo1 = onward(last, ROW)
     pcos, psin = tables(HALF, start - HALF)
     near, log = near_attention(device.reshape(1), cosine, sine, pcos, psin, queries, keys, values, edge)
-    far = plane_attention((device // PLANE).reshape(1), kv2, q2, halo2)
+    far = plane_attention((device // PLANE).reshape(1), held, halo2)
     far = exchange(far)
-    mine, *sent = row_attention(jnp.stack([x[0], device // ROW]), own, others, halo1)
+    mine, *sent = row_attention(jnp.stack([x[0], device // ROW]), pieces, halo1)
     back = [along_row(block, steps) for steps, block in enumerate(sent, 1)]
     attended = merge_groups(x, near, log, far, mine, back)
     other = lax.ppermute(attended, "tp", [(0, 1), (1, 0)])
-    return project(core, attended, other, w_out)
+    partial = project(core, attended, w_out, (), f32)
+    return project(1 - core, other, w_out, (partial,), bf16)
 
 
 def solution(mesh):

time: 120 us -> 125 us (1.042)
  the two profiles are of different devices: /device:TPU:97 before, /device:TPU:8 now
where the time goes in v2:
time: 125 us; the launch traced here: 124 us
  Pallas kernels  35.6 us (28%)
  blocking collectives  27.6 us (22%)
  starting transfers between devices  25.2 us (20%)
  waiting for transfers between devices  23.5 us (19%)
  local copies, waits for them, and re-layouts  8.93 us (7%)
  other arithmetic  3.15 us (3%)
    all_to_all x1, blocking collectives, shards(): held = exchange(held)  27.6 us
    ppermute x6, waiting for transfers between devices, along_row(): lax.ppermute(block, 'sp', [(i, i // ROW * ROW + (i + steps) % ROW) for i...  13.3 us
    ppermute x3, waiting for transfers between devices, onward(): lax.ppermute(block, 'sp', [(i, i + distance) for i in range(devices - dis...  10.2 us
    ppermute x3, starting transfers between devices, onward(): lax.ppermute(block, 'sp', [(i, i + distance) for i in range(devices - dis...  9.97 us
    pallas_call x2, Pallas kernels, project(): pl.pallas_call(project_kernel, in_specs=[pl.BlockSpec(memory_space=pltpu....  8.21 us
    ppermute x6, starting transfers between devices, along_row(): lax.ppermute(block, 'sp', [(i, i // ROW * ROW + (i + steps) % ROW) for i...  8.04 us
    all_to_all x1, starting transfers between devices, shards(): far = exchange(far)  7.07 us
    pallas_call x1, Pallas kernels, row_attention(): pl.pallas_call(row_kernel, in_specs=[pl.BlockSpec(memory_space=pltpu.SMEM...  7 us
  transfers between devices with their start and end apart: 11, of which 5 were waited for; matrix products, arithmetic and copies ran while one was open for 3% of the time, Pallas kernels for 20%

profile of v2, /device:TPU:8, one launch (start us, length us, event | category | flops | bytes accessed | tf_op | source)
XLA Modules:
  0.0 124.3 jit_solution(11306199816772072948)
XLA Ops:
  0.0 1.2 %multiply_sine_fusion = (f32[256,64]{1,0:T(8,128)}, f32[256,64]{1,0:T(8,128)}) fusion(f32[64]{0:T(128)S(1)} %multiply_power_fusion, f32[256]{0:T(256)S(1)} %add_convert_fusion), kind=kLoop, calls=%fused_computation.1 | loop fusion | flops 16384 | bytes 132352 | tf_op jit(solution)/shard_map/sin | solution.py:403
  1.3 4.7 %plane_pieces.1 = bf16[16,3,128,128]{3,2,1,0:T(8,128)(2,1)} custom-call(f32[256,64]{1,0:T(8,128)} %get-tuple-element.26.cos_ref, f32[256,64]{1,0:T(8,128)} %get-tuple-element.25.sin_ref, bf16[3,256,1024]{2,1,0:T(8,128)(2,1)} %k_ref.3, bf16[3,256,1024]{2,1,0:T(8,128)(2,1)} %v_ref.3, bf16[3,256,1024]{2,1,0:T(8,128)(2,1)} %q_ref.3), custom_call_target="tpu_custom_call" | custom-call | flops 1073741824 | bytes 3145728 | tf_op jit(solution)/shard_map/plane_pieces/pallas_call | solution.py:85
  6.0 27.6 %all_to_all.10.in_ref = bf16[16,3,128,128]{3,2,1,0:T(8,128)(2,1)S(1)} all-to-all(bf16[16,3,128,128]{3,2,1,0:T(8,128)(2,1)} %plane_pieces.1), channel_id=1, replica_groups={{0,2,4,6,8,10,12,14,16,18,20,22,24,26,28,30},{32,34,36,38,40,42,44,46,4..., dimensions={0} | all-to-all | bytes 3145728 | tf_op jit(solution)/shard_map/all_to_all | solution.py:427
  33.6 0.8 slice.12
  34.4 4.6 %collective-permute-start.1 = (bf16[8,2,128,128]{3,2,1,0:T(8,128)(2,1)}, bf16[8,2,128,128]{3,2,1,0:T(8,128)(2,1)}, u32[]{:S(2)}, u32[]{:S(2)}) collective-permute-start(bf16[8,2,128,128]{3,2,1,0:T(8,128)(2,1)} %slice.12), channel_id=1, source_target_pairs={{0,32},{2,34},{4,36},{6,38},{8,40},{10,42},{12,44},{14,46},{16,48}... | collective-permute-start | bytes 1572872 | tf_op jit(solution)/shard_map/ppermute | solution.py:418
  39.0 4.3 %row_pieces.1 = (bf16[3,2,256,128]{3,2,1,0:T(8,128)(2,1)}, bf16[3,2,256,128]{3,2,1,0:T(8,128)(2,1)}, bf16[3,2,256,128]{3,2,1,0:T(8,128)(2,1)}, bf16[3,2,256,128]{3,2,1,0:T(8,128)(2,1)}) custom-call(s32[1]{0:T(128)} %bitcast.1.x_ref, f32[256,64]{1,0:T(8,128)} %get-tuple-element.26.cos_ref, f32[256,64]{1,0:T(8,128)} %get-tuple-element.25.sin_ref, ...), custom_call_target="tpu_custom_call" | custom-call | flops 1073741824 | bytes 3145728 | tf_op jit(solution)/shard_map/row_pieces/pallas_call | solution.py:117
  43.4 0.0 copy-start.2
  43.4 0.6 collective-permute-start.2
  44.0 2.5 %collective-permute-start.3 = (bf16[3,2,256,128]{3,2,1,0:T(8,128)(2,1)}, bf16[3,2,256,128]{3,2,1,0:T(8,128)(2,1)S(1)}, u32[]{:S(2)}, u32[]{:S(2)}) collective-permute-start(bf16[3,2,256,128]{3,2,1,0:T(8,128)(2,1)} %get-tuple-element.19), channel_id=1, source_target_pairs={{0,4},{2,6},{4,0},{6,2},{8,12},{10,14},{12,8},{14,10},{16,20},{18,... | collective-permute-start | bytes 1179656 | tf_op jit(solution)/shard_map/ppermute | solution.py:415
  46.5 1.7 %collective-permute-start.4 = (bf16[3,2,256,128]{3,2,1,0:T(8,128)(2,1)}, bf16[3,2,256,128]{3,2,1,0:T(8,128)(2,1)S(1)}, u32[]{:S(2)}, u32[]{:S(2)}) collective-permute-start(bf16[3,2,256,128]{3,2,1,0:T(8,128)(2,1)} %get-tuple-element.20), channel_id=1, source_target_pairs={{0,6},{2,0},{4,2},{6,4},{8,14},{10,8},{12,10},{14,12},{16,22},{18,... | collective-permute-start | bytes 1179656 | tf_op jit(solution)/shard_map/ppermute | solution.py:415
  48.2 1.0 slice.10
  49.1 1.0 slice.9
  50.1 0.8 pad_maximum_fusion
  51.0 2.2 %collective-permute-start = (bf16[2,128,1024]{2,1,0:T(8,128)(2,1)}, bf16[2,128,1024]{2,1,0:T(8,128)(2,1)}, u32[]{:S(2)}, u32[]{:S(2)}) collective-permute-start(bf16[2,128,1024]{2,1,0:T(8,128)(2,1)} %pad_maximum_fusion), channel_id=1, source_target_pairs={{0,2},{2,4},{4,6},{6,8},{8,10},{10,12},{12,14},{14,16},{16,18},{18... | collective-permute-start | bytes 1572872 | tf_op jit(solution)/shard_map/ppermute | solution.py:418
  53.2 11.2 %collective-permute-done.2.one_ref = bf16[3,2,256,128]{3,2,1,0:T(8,128)(2,1)S(1)} collective-permute-done((bf16[3,2,256,128]{3,2,1,0:T(8,128)(2,1)}, bf16[3,2,256,128]{3,2,1,0:T(8,128)(2,1)S(1)}, u32[]{:S(2)}, u32[]{:S(2)}) %collective-permute-start.2) | collective-permute-done | bytes 393248 | tf_op jit(solution)/shard_map/ppermute | solution.py:415
  64.4 0.8 collective-permute-done.3.two_ref
  65.1 0.0 collective-permute-done.4.three_ref
  65.1 0.0 copy-start.3
  65.1 0.7 copy-done.3
  65.9 0.0 copy-done.2
  65.9 0.0 copy-start.4
  65.9 1.0 copy-done.4
  66.9 3.1 %collective-permute-start.5 = (bf16[2,2,2,256,128]{4,3,2,1,0:T(8,128)(2,1)S(1)}, bf16[2,2,2,256,128]{4,3,2,1,0:T(8,128)(2,1)}, u32[]{:S(2)}, u32[]{:S(2)}) collective-permute-start(bf16[2,2,2,256,128]{4,3,2,1,0:T(8,128)(2,1)S(1)} %pick_last.1), channel_id=1, source_target_pairs={{0,8},{2,10},{4,12},{6,14},{8,16},{10,18},{12,20},{14,22},{16,24},... | collective-permute-start | bytes 1572872 | tf_op jit(solution)/shard_map/ppermute | solution.py:418
  70.1 0.0 collective-permute-done.1.halo_ref
  70.1 3.6 %plane_attention.1 = bf16[16,144,128]{2,1,0:T(8,128)(2,1)} custom-call(s32[1]{0:T(128)} %bitcast.3.z_ref, bf16[16,3,128,128]{3,2,1,0:T(8,128)(2,1)S(1)} %all_to_all.10.in_ref, bf16[8,2,128,128]{3,2,1,0:T(8,128)(2,1)} %collective-permute-done.1.halo_ref), custom_call_target="tpu_custom_call" | custom-call | flops 2147483648 | bytes 3145728 | tf_op jit(solution)/shard_map/plane_attention/pallas_call | solution.py:193
  73.7 7.1 %all-to-all-start.1 = ((bf16[16,144,128]{2,1,0:T(8,128)(2,1)}), bf16[16,144,128]{2,1,0:T(8,128)(2,1)S(1)}, u32[]{:S(2)}, u32[]{:S(2)}) async-start(bf16[16,144,128]{2,1,0:T(8,128)(2,1)} %plane_attention.1), calls=%async_computation.1 | async-start | bytes 1179648 | tf_op jit(solution)/shard_map/all_to_all | solution.py:437
  80.8 1.0 multiply_sine_fusion.1
  81.7 0.1 pad_add_fusion.x_ref
  81.8 10.2 %collective-permute-done.5.halo_ref = bf16[2,2,2,256,128]{4,3,2,1,0:T(8,128)(2,1)} collective-permute-done((bf16[2,2,2,256,128]{4,3,2,1,0:T(8,128)(2,1)S(1)}, bf16[2,2,2,256,128]{4,3,2,1,0:T(8,128)(2,1)}, u32[]{:S(2)}, u32[]{:S(2)}) %collective-permute-start.5) | collective-permute-done | bytes 524320 | tf_op jit(solution)/shard_map/ppermute | solution.py:418
  92.0 0.0 copy-start.5
  92.0 1.0 copy-done.5
  93.0 7.0 %row_attention.1 = (bf16[2,272,128]{2,1,0:T(8,128)(2,1)S(1)}, bf16[2,272,128]{2,1,0:T(8,128)(2,1)S(1)}, bf16[2,272,128]{2,1,0:T(8,128)(2,1)S(1)}, bf16[2,272,128]{2,1,0:T(8,128)(2,1)S(1)}) custom-call(s32[2]{0:T(128)S(1)} %pad_add_fusion.x_ref, bf16[3,2,256,128]{3,2,1,0:T(8,128)(2,1)S(1)} %copy-done.2, ...), custom_call_target="tpu_custom_call" | custom-call | flops 2147483648 | bytes 3145728 | tf_op jit(solution)/shard_map/row_attention/pallas_call | solution.py:263
  100.0 0.0 collective-permute-start.6
  100.0 0.1 collective-permute-start.7
  100.1 3.1 %collective-permute-start.8 = (bf16[2,272,128]{2,1,0:T(8,128)(2,1)S(1)}, bf16[2,272,128]{2,1,0:T(8,128)(2,1)S(1)}, u32[]{:S(2)}, u32[]{:S(2)}) collective-permute-start(bf16[2,272,128]{2,1,0:T(8,128)(2,1)S(1)} %get-tuple-element.24), channel_id=1, source_target_pairs={{0,6},{2,0},{4,2},{6,4},{8,14},{10,8},{12,10},{14,12},{16,22},{18,... | collective-permute-start | bytes 417800 | tf_op jit(solution)/shard_map/ppermute | solution.py:415
  103.3 0.0 collective-permute-done.halo_ref
  103.3 5.7 %near_attention.1 = (bf16[256,1024]{1,0:T(8,128)(2,1)}, f32[256,128]{1,0:T(8,128)}) custom-call(s32[1]{0:T(128)} %bitcast.2.z_ref, f32[256,64]{1,0:T(8,128)} %get-tuple-element.26.cos_ref, f32[256,64]{1,0:T(8,128)} %get-tuple-element.25.sin_ref, f32[128,64]{1,0:T(8,128)} %get-tuple-element.28.pcos_ref, f32[128,64]{1,0:T(8,128)} %get-tuple-element.27.psin_ref, ...), custom_call_target="tpu_custom_call" | custom-call | flops 2147483648 | bytes 4194304 | tf_op jit(solution)/shard_map/near_attention/pallas_call | solution.py:313
  108.9 0.8 collective-permute-done.6.one_ref
  109.7 0.0 collective-permute-done.7.two_ref
  109.7 0.6 collective-permute-done.8.three_ref
  110.3 0.0 all-to-all-done.1.far_ref
  110.3 0.0 copy-start.1
  110.3 1.0 copy-done.1
  111.4 0.0 copy-start.6
  111.4 0.9 copy-done.6
  112.3 2.0 %merge_groups.1.in_ref = bf16[256,1024]{1,0:T(8,128)(2,1)S(1)} custom-call(s32[1]{0:T(128)} %bitcast.1.x_ref, bf16[256,1024]{1,0:T(8,128)(2,1)S(1)} %copy-done.1, f32[256,128]{1,0:T(8,128)S(1)} %copy-done.6, bf16[16,144,128]{2,1,0:T(8,128)(2,1)S(1)} %all-to-all-done.1.far_ref, bf16[2,272,128]{2,1,0:T(8,128)(2,1)S(1)} %get-tuple-element.21.own_ref, ...), custom_call_target="tpu_custom_call" | custom-call | flops 16777216 | bytes 2097152 | tf_op jit(solution)/shard_map/merge_groups/pallas_call | solution.py:356
  114.3 0.0 copy-start
  114.3 0.1 collective-permute-start.9
  114.4 0.7 copy-done
  115.1 4.1 %project.2.refs_0_ = f32[256,1024]{1,0:T(8,128)} custom-call(s32[1]{0:T(128)} %bitcast.start_ref, bf16[256,1024]{1,0:T(8,128)(2,1)} %copy-done, bf16[2048,1024]{1,0:T(8,128)(2,1)} %w_hbm.3), custom_call_target="tpu_custom_call" | custom-call | flops 536870912 | bytes 4194304 | tf_op jit(solution)/shard_map/project/pallas_call | solution.py:388
  119.2 0.0 collective-permute-done.9.in_ref
  119.2 0.0 copy-start.7
  119.2 0.8 copy-done.7
  120.0 4.1 %project.3 = bf16[256,1024]{1,0:T(8,128)(2,1)} custom-call(s32[1]{0:T(128)S(6)} %sub.13.start_ref, bf16[256,1024]{1,0:T(8,128)(2,1)} %copy-done.7, bf16[2048,1024]{1,0:T(8,128)(2,1)} %w_hbm.3, f32[256,1024]{1,0:T(8,128)} %project.2.refs_0_), custom_call_target="tpu_custom_call" | custom-call | flops 536870912 | bytes 4194304 | tf_op jit(solution)/shard_map/project/pallas_call | solution.py:388
  (4 shorter events, 0.1 us)
Async XLA Ops:
  34.4 35.7 %collective-permute-start.1 = (bf16[8,2,128,128]{3,2,1,0:T(8,128)(2,1)}, bf16[8,2,128,128]{3,2,1,0:T(8,128)(2,1)}, u32[]{:S(2)}, u32[]{:S(2)}) collective-permute-start(bf16[8,2,128,128]{3,2,1,0:T(8,128)(2,1)} %slice.12), channel_id=1, source_target_pairs={{0,32},{2,34},{4,36},{6,38},{8,40},{10,42},{12,44},{14,46},{16,48}... | collective-permute-start | bytes 1572872 | tf_op jit(solution)/shard_map/ppermute | solution.py:418
  43.4 22.5 %copy-start.2 = (bf16[3,2,256,128]{3,2,1,0:T(8,128)(2,1)S(1)}, bf16[3,2,256,128]{3,2,1,0:T(8,128)(2,1)}, u32[]{:S(2)}) copy-start(bf16[3,2,256,128]{3,2,1,0:T(8,128)(2,1)} %get-tuple-element.17.own_ref) | copy-start | bytes 1179652
  43.4 21.0 %collective-permute-start.2 = (bf16[3,2,256,128]{3,2,1,0:T(8,128)(2,1)}, bf16[3,2,256,128]{3,2,1,0:T(8,128)(2,1)S(1)}, u32[]{:S(2)}, u32[]{:S(2)}) collective-permute-start(bf16[3,2,256,128]{3,2,1,0:T(8,128)(2,1)} %get-tuple-element.18), channel_id=1, source_target_pairs={{0,2},{2,4},{4,6},{6,0},{8,10},{10,12},{12,14},{14,8},{16,18},{18,... | collective-permute-start | bytes 1179656 | tf_op jit(solution)/shard_map/ppermute | solution.py:415
  44.0 21.1 %collective-permute-start.3 = (bf16[3,2,256,128]{3,2,1,0:T(8,128)(2,1)}, bf16[3,2,256,128]{3,2,1,0:T(8,128)(2,1)S(1)}, u32[]{:S(2)}, u32[]{:S(2)}) collective-permute-start(bf16[3,2,256,128]{3,2,1,0:T(8,128)(2,1)} %get-tuple-element.19), channel_id=1, source_target_pairs={{0,4},{2,6},{4,0},{6,2},{8,12},{10,14},{12,8},{14,10},{16,20},{18,... | collective-permute-start | bytes 1179656 | tf_op jit(solution)/shard_map/ppermute | solution.py:415
  46.5 18.7 %collective-permute-start.4 = (bf16[3,2,256,128]{3,2,1,0:T(8,128)(2,1)}, bf16[3,2,256,128]{3,2,1,0:T(8,128)(2,1)S(1)}, u32[]{:S(2)}, u32[]{:S(2)}) collective-permute-start(bf16[3,2,256,128]{3,2,1,0:T(8,128)(2,1)} %get-tuple-element.20), channel_id=1, source_target_pairs={{0,6},{2,0},{4,2},{6,4},{8,14},{10,8},{12,10},{14,12},{16,22},{18,... | collective-permute-start | bytes 1179656 | tf_op jit(solution)/shard_map/ppermute | solution.py:415
  51.0 52.3 %collective-permute-start = (bf16[2,128,1024]{2,1,0:T(8,128)(2,1)}, bf16[2,128,1024]{2,1,0:T(8,128)(2,1)}, u32[]{:S(2)}, u32[]{:S(2)}) collective-permute-start(bf16[2,128,1024]{2,1,0:T(8,128)(2,1)} %pad_maximum_fusion), channel_id=1, source_target_pairs={{0,2},{2,4},{4,6},{6,8},{8,10},{10,12},{12,14},{14,16},{16,18},{18... | collective-permute-start | bytes 1572872 | tf_op jit(solution)/shard_map/ppermute | solution.py:418
  65.1 0.7 copy-start.3
  65.9 1.0 copy-start.4
  66.9 25.1 %collective-permute-start.5 = (bf16[2,2,2,256,128]{4,3,2,1,0:T(8,128)(2,1)S(1)}, bf16[2,2,2,256,128]{4,3,2,1,0:T(8,128)(2,1)}, u32[]{:S(2)}, u32[]{:S(2)}) collective-permute-start(bf16[2,2,2,256,128]{4,3,2,1,0:T(8,128)(2,1)S(1)} %pick_last.1), channel_id=1, source_target_pairs={{0,8},{2,10},{4,12},{6,14},{8,16},{10,18},{12,20},{14,22},{16,24},... | collective-permute-start | bytes 1572872 | tf_op jit(solution)/shard_map/ppermute | solution.py:418
  73.7 36.7 %all-to-all-start.1 = ((bf16[16,144,128]{2,1,0:T(8,128)(2,1)}), bf16[16,144,128]{2,1,0:T(8,128)(2,1)S(1)}, u32[]{:S(2)}, u32[]{:S(2)}) async-start(bf16[16,144,128]{2,1,0:T(8,128)(2,1)} %plane_attention.1), calls=%async_computation.1 | async-start | bytes 1179648 | tf_op jit(solution)/shard_map/all_to_all | solution.py:437
  92.0 1.0 copy-start.5
  100.0 9.7 %collective-permute-start.6 = (bf16[2,272,128]{2,1,0:T(8,128)(2,1)S(1)}, bf16[2,272,128]{2,1,0:T(8,128)(2,1)S(1)}, u32[]{:S(2)}, u32[]{:S(2)}) collective-permute-start(bf16[2,272,128]{2,1,0:T(8,128)(2,1)S(1)} %get-tuple-element.22), channel_id=1, source_target_pairs={{0,2},{2,4},{4,6},{6,0},{8,10},{10,12},{12,14},{14,8},{16,18},{18,... | collective-permute-start | bytes 417800 | tf_op jit(solution)/shard_map/ppermute | solution.py:415
  100.0 9.7 %collective-permute-start.7 = (bf16[2,272,128]{2,1,0:T(8,128)(2,1)S(1)}, bf16[2,272,128]{2,1,0:T(8,128)(2,1)S(1)}, u32[]{:S(2)}, u32[]{:S(2)}) collective-permute-start(bf16[2,272,128]{2,1,0:T(8,128)(2,1)S(1)} %get-tuple-element.23), channel_id=1, source_target_pairs={{0,4},{2,6},{4,0},{6,2},{8,12},{10,14},{12,8},{14,10},{16,20},{18,... | collective-permute-start | bytes 417800 | tf_op jit(solution)/shard_map/ppermute | solution.py:415
  100.1 10.2 %collective-permute-start.8 = (bf16[2,272,128]{2,1,0:T(8,128)(2,1)S(1)}, bf16[2,272,128]{2,1,0:T(8,128)(2,1)S(1)}, u32[]{:S(2)}, u32[]{:S(2)}) collective-permute-start(bf16[2,272,128]{2,1,0:T(8,128)(2,1)S(1)} %get-tuple-element.24), channel_id=1, source_target_pairs={{0,6},{2,0},{4,2},{6,4},{8,14},{10,8},{12,10},{14,12},{16,22},{18,... | collective-permute-start | bytes 417800 | tf_op jit(solution)/shard_map/ppermute | solution.py:415
  110.3 1.0 copy-start.1
  111.4 0.9 copy-start.6
  114.3 0.8 copy-start
  114.3 4.9 %collective-permute-start.9 = (bf16[256,1024]{1,0:T(8,128)(2,1)S(1)}, bf16[256,1024]{1,0:T(8,128)(2,1)S(1)}, u32[]{:S(2)}, u32[]{:S(2)}) collective-permute-start(bf16[256,1024]{1,0:T(8,128)(2,1)S(1)} %merge_groups.1.in_ref), channel_id=1, source_target_pairs={{0,1},{1,0},{2,3},{3,2},{4,5},{5,4},{6,7},{7,6},{8,9},{9,8},{10,11... | collective-permute-start | bytes 1572872 | tf_op jit(solution)/shard_map/ppermute | solution.py:441
  119.2 0.8 copy-start.7

commit v3 on v2

--- a/solution.py
+++ b/solution.py
@@ -20,7 +20,6 @@
 HALF = TOKENS // 2
 ROW = 4
 ROW_HEADS = LOCAL // ROW
-STRIDES = {1: 4, 2: 16}
 RETURN_ROWS = HALF + 16
 ROW_RETURN = TOKENS + 16
 
@@ -43,86 +42,103 @@
     return jnp.concatenate([cosine, cosine], axis=1), jnp.concatenate([-sine, sine], axis=1)
 
 
-def sorting(group):
-    row = iota((TOKENS, TOKENS), 0)
-    token = iota((TOKENS, TOKENS), 1)
-    stride = STRIDES[group]
-    shift = (TOKENS // stride).bit_length() - 1
-    step = row & (2**shift - 1)
-    if group == 2:
-        picked = (row >> 7) + 2 * ((row & (HALF - 1)) >> shift) + stride * step
-    else:
-        picked = (row >> shift) + stride * step
-    return jnp.where(picked == token, 1.0, 0.0).astype(bf16)
-
-
-def load_kind(kind, x, cosine, sine):
+def fetched(sources, target, sem):
+    copies = [pltpu.make_async_copy(ref, target.at[a], sem.at[a]) for a, ref in enumerate(sources)]
+    for copy in copies:
+        copy.start()
+    return copies
+
+
+def turned_as(kind, x, cosine, sine):
     if kind == "v":
-        return x
-    heads = [turned(x[:, h * HEAD : (h + 1) * HEAD], cosine, sine) for h in range(2)]
-    if kind == "q":
-        heads = [x * SCALE for x in heads]
-    return jnp.concatenate([x.astype(bf16) for x in heads], axis=1)
-
-
-def plane_pieces_kernel(cos_ref, sin_ref, k_ref, v_ref, q_ref, out_ref, sort_ref, full_ref):
-    @pl.when(pl.program_id(0) == 0)
-    def _():
-        sort_ref[...] = sorting(2)
-        full_ref[0], full_ref[1] = full_tables(cos_ref, sin_ref)
-
-    cosine, sine = full_ref[0], full_ref[1]
-    for a, (kind, ref) in enumerate((("k", k_ref), ("v", v_ref), ("q", q_ref))):
-        x = load_kind(kind, ref[...], cosine, sine)
-        y = jnp.dot(sort_ref[...], x, preferred_element_type=f32).astype(bf16)
-        for h in range(2):
+        return x.astype(f32)
+    return turned(x, cosine, sine) * (SCALE if kind == "q" else 1.0)
+
+
+def plane_pieces_kernel(cos_ref, sin_ref, k_ref, v_ref, q_ref, out_ref, in_ref, sort_ref, piece_ref, sem, out_sem):
+    copies = fetched([ref.at[2] for ref in (k_ref, v_ref, q_ref)], in_ref, sem)
+    cosine, sine = full_tables(cos_ref, sin_ref)
+    stores = []
+    for a, kind in enumerate("kvq"):
+        copies[a].wait()
+        for h in range(LOCAL):
+            sort_ref[h] = turned_as(kind, in_ref[a, :, h * HEAD : (h + 1) * HEAD], cosine, sine)
             for p in range(2):
-                out_ref[2 * h + p, a] = y[p * HALF : (p + 1) * HALF, h * HEAD : (h + 1) * HEAD]
+                rows = [sort_ref[h, pl.ds(p + 2 * r, 16, stride=16), :] for r in range(8)]
+                piece_ref[2 * h + p, a] = jnp.concatenate(rows, axis=0).astype(bf16)
+        stores.append(pltpu.make_async_copy(piece_ref.at[:, a], out_ref.at[:, a], out_sem.at[a]))
+        stores[-1].start()
+    for store in stores:
+        store.wait()
 
 
 def plane_pieces(keys, values, queries, cosine, sine):
-    table = pl.BlockSpec((TOKENS, HEAD // 2), lambda g: (0, 0))
+    vmem, hbm = pl.BlockSpec(memory_space=pltpu.VMEM), pl.BlockSpec(memory_space=pltpu.HBM)
+    shape = (PLANE, 3, HALF, HEAD)
     return pl.pallas_call(
         plane_pieces_kernel,
-        grid=(LOCAL // 2,),
-        in_specs=[table, table] + [pl.BlockSpec((None, TOKENS, 2 * HEAD), lambda g: (2, 0, g))] * 3,
-        out_specs=pl.BlockSpec((4, 3, HALF, HEAD), lambda g: (g, 0, 0, 0)),
-        scratch_shapes=[pltpu.VMEM((TOKENS, TOKENS), bf16), pltpu.VMEM((2, TOKENS, HEAD), f32)],
-        out_shape=jax.ShapeDtypeStruct((PLANE, 3, HALF, HEAD), bf16),
+        in_specs=[vmem, vmem, hbm, hbm, hbm],
+        out_specs=hbm,
+        scratch_shapes=[
+            pltpu.VMEM((3, TOKENS, LOCAL * HEAD), bf16),
+            pltpu.VMEM((LOCAL, TOKENS, HEAD), f32),
+            pltpu.VMEM(shape, bf16),
+            pltpu.SemaphoreType.DMA((3,)),
+            pltpu.SemaphoreType.DMA((3,)),
+        ],
+        out_shape=jax.ShapeDtypeStruct(shape, bf16),
         cost_estimate=pl.CostEstimate(flops=2**30, bytes_accessed=3 * 2**20, transcendentals=0),
         name="plane_pieces",
     )(cosine, sine, keys, values, queries)
 
 
 def row_pieces_kernel(x_ref, cos_ref, sin_ref, k_ref, v_ref, q_ref, *refs):
-    outs, in_ref, sem = refs[:ROW], refs[ROW], refs[ROW + 1]
-    copies = [pltpu.make_async_copy(ref.at[1], in_ref.at[a], sem.at[a]) for a, ref in enumerate((k_ref, v_ref, q_ref))]
-    for copy in copies:
-        copy.start()
-    sort = sorting(1)
+    outs, halos = refs[:ROW], refs[ROW : 2 * ROW]
+    in_ref, sort_ref, piece_ref, sem, out_sem = refs[2 * ROW :]
+    copies = fetched([ref.at[1] for ref in (k_ref, v_ref, q_ref)], in_ref, sem)
     cosine, sine = full_tables(cos_ref, sin_ref)
-    width = ROW_HEADS * HEAD
+    stores = []
+
+    def store(source, target, index):
+        stores.append(pltpu.make_async_copy(source, target, out_sem.at[index]))
+        stores[-1].start()
+
     for a, kind in enumerate("kvq"):
         copies[a].wait()
         for steps in range(ROW):
             chip = lax.rem(x_ref[0] + steps, ROW)
-            x = in_ref[a, :, pl.ds(pl.multiple_of(chip * width, width), width)]
-            y = jnp.dot(sort, load_kind(kind, x, cosine, sine), preferred_element_type=f32).astype(bf16)
             for h in range(ROW_HEADS):
-                outs[steps][a, h] = y[:, h * HEAD : (h + 1) * HEAD]
+                lanes = pl.ds(pl.multiple_of((chip * ROW_HEADS + h) * HEAD, HEAD), HEAD)
+                slot = steps * ROW_HEADS + h
+                sort_ref[slot] = turned_as(kind, in_ref[a, :, lanes], cosine, sine)
+                rows = [sort_ref[slot, pl.ds(r, 64, stride=4), :] for r in range(4)]
+                piece_ref[steps, a, h] = jnp.concatenate(rows, axis=0).astype(bf16)
+            store(piece_ref.at[steps, a], outs[steps].at[a], a * ROW + steps)
+            if kind != "q":
+                store(piece_ref.at[steps, a], halos[steps].at[a], (3 + a) * ROW + steps)
+    for copy in stores:
+        copy.wait()
 
 
 def row_pieces(x, keys, values, queries, cosine, sine):
     vmem, hbm = pl.BlockSpec(memory_space=pltpu.VMEM), pl.BlockSpec(memory_space=pltpu.HBM)
-    return pl.pallas_call(
+    shape = (ROW_HEADS, TOKENS, HEAD)
+    outs = pl.pallas_call(
         row_pieces_kernel,
         in_specs=[pl.BlockSpec(memory_space=pltpu.SMEM), vmem, vmem, hbm, hbm, hbm],
-        out_specs=[vmem] * ROW,
-        scratch_shapes=[pltpu.VMEM((3, TOKENS, LOCAL * HEAD), bf16), pltpu.SemaphoreType.DMA((3,))],
-        out_shape=[jax.ShapeDtypeStruct((3, ROW_HEADS, TOKENS, HEAD), bf16)] * ROW,
+        out_specs=[hbm] * (2 * ROW),
+        scratch_shapes=[
+            pltpu.VMEM((3, TOKENS, LOCAL * HEAD), bf16),
+            pltpu.VMEM((LOCAL, TOKENS, HEAD), f32),
+            pltpu.VMEM((ROW, 3, *shape), bf16),
+            pltpu.SemaphoreType.DMA((3,)),
+            pltpu.SemaphoreType.DMA((5 * ROW,)),
+        ],
+        out_shape=[jax.ShapeDtypeStruct((3, *shape), bf16)] * ROW + [jax.ShapeDtypeStruct((2, *shape), bf16)] * ROW,
         cost_estimate=pl.CostEstimate(flops=2**30, bytes_accessed=3 * 2**20, transcendentals=0),
         name="row_pieces",
     )(x, cosine, sine, keys, values, queries)
+    return list(outs[:ROW]), list(outs[ROW:])
 
 
 def dot_t(a, b):
@@ -202,35 +218,19 @@
     )(z, held, halo)
 
 
-def pick_kernel(x_ref, own_ref, one_ref, two_ref, three_ref, out_ref):
-    x = x_ref[0]
-    for steps, ref in enumerate((own_ref, one_ref, two_ref, three_ref)):
-        chip = lax.rem(x + ROW - steps, ROW)
-
-        @pl.when(chip >= ROW // 2)
-        def _(ref=ref, chip=chip):
-            out_ref[chip - ROW // 2] = ref[:2]
-
-
-def pick_last(x, pieces):
-    vmem = pl.BlockSpec(memory_space=pltpu.VMEM)
-    return pl.pallas_call(
-        pick_kernel,
-        in_specs=[pl.BlockSpec(memory_space=pltpu.SMEM)] + [vmem] * ROW,
-        out_specs=vmem,
-        out_shape=jax.ShapeDtypeStruct((2, 2, ROW_HEADS, TOKENS, HEAD), bf16),
-        compiler_params=pltpu.CompilerParams(vmem_limit_bytes=4 * 2**20),
-        cost_estimate=pl.CostEstimate(flops=2**20, bytes_accessed=2**21, transcendentals=0),
-        name="pick_last",
-    )(x, *pieces)
-
-
-def row_kernel(x_ref, own_ref, one_ref, two_ref, three_ref, halo_ref, *refs):
-    outs, in_ref, res_ref = refs[:4], *refs[4:]
+def row_kernel(x_ref, *refs):
+    ins, halos, outs = refs[:ROW], refs[ROW : 2 * ROW], refs[2 * ROW : 3 * ROW]
+    in_ref, halo_ref, res_ref, logs_ref = refs[3 * ROW :]
     x = x_ref[0]
     bias = jnp.where(x_ref[1] == 0, MASKED, -MASKED)
-    for steps, ref in enumerate((own_ref, one_ref, two_ref, three_ref)):
-        in_ref[lax.rem(x + ROW - steps, ROW)] = ref[...]
+    for steps in range(ROW):
+        chip = lax.rem(x + ROW - steps, ROW)
+        in_ref[chip] = ins[steps][...]
+
+        @pl.when(chip >= ROW // 2)
+        def _(steps=steps, chip=chip):
+            halo_ref[chip - ROW // 2] = halos[steps][...]
+
     for h in range(ROW_HEADS):
         for r in range(4):
             rows = slice(r * 64, (r + 1) * 64)
@@ -242,37 +242,36 @@
                 vs.append(jnp.concatenate([in_ref[s, 1, h, rows, :] for s in chips], axis=0))
                 q = jnp.concatenate([in_ref[s, 2, h, rows, :] for s in chips], axis=0)
                 result, logs = attend(q, ks[b], ks[b + 1], vs[b], vs[b + 1], bias if b == 0 else None)
-                tile = column_to_rows(logs)
                 for i, s in enumerate(chips):
                     res_ref[s, h, rows, :] = result[i * 64 : (i + 1) * 64].astype(bf16)
-                    half = tile if i == 0 else pltpu.roll(tile, HEAD // 2, 1)
-                    sub = iota((16, HEAD), 0)
-                    held = half if r == 0 else jnp.where(sub // 2 == r, half, carried[i + 2 * b])
-                    if r == 0 and b == 0 and i == 0:
-                        carried = {}
-                    carried[i + 2 * b] = held
-                    if r == 3:
-                        res_ref[s, h, TOKENS:, :] = held.astype(bf16)
+                    logs_ref[s, h, rows, :] = logs[i * 64 : (i + 1) * 64]
+    sub = iota((16, HEAD), 0)
+    for s in range(ROW):
+        for h in range(ROW_HEADS):
+            tiles = [column_to_rows(logs_ref[s, h, half * HALF : (half + 1) * HALF, :]) for half in range(2)]
+            res_ref[s, h, TOKENS:, :] = jnp.where(sub < 2, tiles[0], tiles[1]).astype(bf16)
     for steps, out in enumerate(outs):
         out[...] = res_ref[lax.rem(x + steps, ROW)]
 
 
-def row_attention(place, pieces, halo):
+def row_attention(place, pieces, halos):
     shape = (ROW_HEADS, ROW_RETURN, HEAD)
     vmem = pl.BlockSpec(memory_space=pltpu.VMEM)
     return pl.pallas_call(
         row_kernel,
-        in_specs=[pl.BlockSpec(memory_space=pltpu.SMEM)] + [vmem] * (ROW + 1),
+        in_specs=[pl.BlockSpec(memory_space=pltpu.SMEM)] + [vmem] * (2 * ROW),
         out_specs=[vmem] * ROW,
         out_shape=[jax.ShapeDtypeStruct(shape, bf16)] * ROW,
         scratch_shapes=[
             pltpu.VMEM((ROW, 3, ROW_HEADS, TOKENS, HEAD), bf16),
+            pltpu.VMEM((2, 2, ROW_HEADS, TOKENS, HEAD), bf16),
             pltpu.VMEM((ROW, *shape), bf16),
+            pltpu.VMEM((ROW, ROW_HEADS, TOKENS, 1), f32),
         ],
-        compiler_params=pltpu.CompilerParams(vmem_limit_bytes=10 * 2**20),
+        compiler_params=pltpu.CompilerParams(vmem_limit_bytes=12 * 2**20),
         cost_estimate=pl.CostEstimate(flops=2**31, bytes_accessed=3 * 2**20, transcendentals=2**19),
         name="row_attention",
-    )(place, *pieces, halo)
+    )(place, *pieces, *halos)
 
 
 def near_kernel(
@@ -338,12 +337,14 @@
                 far[h % 2, target, :] = far_ref[piece, r * 16 : (r + 1) * 16, :].astype(f32)
                 far_log[h % 2, target, :] = logs[r * 16 : (r + 1) * 16]
         chip, head = h // ROW_HEADS, h % ROW_HEADS
-        for r in range(4):
-            target = pl.ds(r, 64, stride=4)
-            rows = TOKENS + 2 * r
+        for half in range(2):
+            rows = TOKENS + 2 * half
             logs = rows_to_column(row_ref[chip, head, rows : rows + 1, :], row_ref[chip, head, rows + 1 : rows + 2, :])
-            mid[h % 2, target, :] = row_ref[chip, head, r * 64 : (r + 1) * 64, :].astype(f32)
-            mid_log[h % 2, target, :] = logs[:64]
+            for i in range(2):
+                r = 2 * half + i
+                target = pl.ds(r, 64, stride=4)
+                mid[h % 2, target, :] = row_ref[chip, head, r * 64 : (r + 1) * 64, :].astype(f32)
+                mid_log[h % 2, target, :] = logs[i * 64 : (i + 1) * 64]
         logs = [wide(log_ref[:, h : h + 1]), mid_log[h % 2], far_log[h % 2]]
         top = jnp.maximum(jnp.maximum(logs[0], logs[1]), logs[2])
         e = [jnp.exp(x - top) for x in logs]
@@ -352,6 +353,7 @@
 
 
 def merge_groups(x, near, log, far, own, others):
+
     vmem = pl.BlockSpec(memory_space=pltpu.VMEM)
     return pl.pallas_call(
         merge_kernel,
@@ -365,36 +367,27 @@
     )(x, near, log, far, own, *others)
 
 
-def project_kernel(start_ref, in_ref, w_hbm, *refs):
-    *partial, out_ref, w_ref, sem = refs
+def project_kernel(core_ref, mine_ref, other_ref, w_ref, out_ref):
     half = LOCAL * HEAD
-    chunk = half // 4
-    copies = []
-    for c in range(4):
-        rows = pl.ds(pl.multiple_of(start_ref[0] * half + c * chunk, chunk), chunk)
-        copies.append(pltpu.make_async_copy(w_hbm.at[rows], w_ref.at[pl.ds(c * chunk, chunk)], sem.at[c]))
-        copies[-1].start()
-    total = partial[0][...] if partial else None
-    for c in range(4):
-        copies[c].wait()
-        part = slice(c * chunk, (c + 1) * chunk)
-        term = jnp.dot(in_ref[:, part], w_ref[part, :], preferred_element_type=f32)
-        total = term if total is None else total + term
-    out_ref[...] = total.astype(out_ref.dtype)
-
-
-def project(core, block, w_out, partial, dtype):
-    vmem, hbm = pl.BlockSpec(memory_space=pltpu.VMEM), pl.BlockSpec(memory_space=pltpu.HBM)
+    core = core_ref[0]
+    mine = pl.ds(pl.multiple_of(core * half, half), half)
+    other = pl.ds(pl.multiple_of((1 - core) * half, half), half)
+    total = jnp.dot(mine_ref[...], w_ref[mine, :], preferred_element_type=f32)
+    total += jnp.dot(other_ref[...], w_ref[other, :], preferred_element_type=f32)
+    out_ref[...] = total.astype(bf16)
+
+
+def project(core, mine, other, w_out):
+    vmem = pl.BlockSpec(memory_space=pltpu.VMEM)
     return pl.pallas_call(
         project_kernel,
-        in_specs=[pl.BlockSpec(memory_space=pltpu.SMEM), vmem, hbm] + [vmem] * len(partial),
+        in_specs=[pl.BlockSpec(memory_space=pltpu.SMEM), vmem, vmem, vmem],
         out_specs=vmem,
-        out_shape=jax.ShapeDtypeStruct((TOKENS, w_out.shape[1]), dtype),
-        scratch_shapes=[pltpu.VMEM((LOCAL * HEAD, w_out.shape[1]), bf16), pltpu.SemaphoreType.DMA((4,))],
-        compiler_params=pltpu.CompilerParams(vmem_limit_bytes=58 * 2**20),
-        cost_estimate=pl.CostEstimate(flops=2**29, bytes_accessed=2**22, transcendentals=0),
+        out_shape=jax.ShapeDtypeStruct((TOKENS, w_out.shape[1]), bf16),
+        compiler_params=pltpu.CompilerParams(vmem_limit_bytes=8 * 2**20),
+        cost_estimate=pl.CostEstimate(flops=2**30, bytes_accessed=2**22, transcendentals=0),
         name="project",
-    )(core, block, w_out, *partial)
+    )(core, mine, other, w_out)
 
 
 def tables(count, start):
@@ -414,6 +407,10 @@
     def along_row(block, steps):
         return lax.ppermute(block, "sp", [(i, i // ROW * ROW + (i + steps) % ROW) for i in range(devices)])
 
+    def to_next_row(block, steps):
+        sources = [i for i in range(devices - ROW) if i % ROW >= ROW // 2]
+        return lax.ppermute(block, "sp", [(i, (i // ROW + 1) * ROW + (i + steps) % ROW) for i in sources])
+
     def onward(block, distance):
         return lax.ppermute(block, "sp", [(i, i + distance) for i in range(devices - distance)])
 
@@ -425,22 +422,20 @@
 
     held = plane_pieces(keys, values, queries, cosine, sine)
     held = exchange(held)
-    own, *others = row_pieces(x, keys, values, queries, cosine, sine)
-    pieces = [own] + [along_row(block, steps) for steps, block in enumerate(others, 1)]
+    pieces, halos = row_pieces(x, keys, values, queries, cosine, sine)
+    pieces = pieces[:1] + [along_row(block, steps) for steps, block in enumerate(pieces[1:], 1)]
+    halos = [to_next_row(block, steps) for steps, block in enumerate(halos)]
+    halo2 = onward(held[PLANE // 2 :, :2], PLANE)
     edge = onward(jnp.stack([keys[0, HALF:], values[0, HALF:]]), 1)
-    halo2 = onward(held[PLANE // 2 :, :2], PLANE)
-    last = pick_last(x, pieces)
-    halo1 = onward(last, ROW)
     pcos, psin = tables(HALF, start - HALF)
     near, log = near_attention(device.reshape(1), cosine, sine, pcos, psin, queries, keys, values, edge)
     far = plane_attention((device // PLANE).reshape(1), held, halo2)
     far = exchange(far)
-    mine, *sent = row_attention(jnp.stack([x[0], device // ROW]), pieces, halo1)
+    mine, *sent = row_attention(jnp.stack([x[0], device // ROW]), pieces, halos)
     back = [along_row(block, steps) for steps, block in enumerate(sent, 1)]
     attended = merge_groups(x, near, log, far, mine, back)
     other = lax.ppermute(attended, "tp", [(0, 1), (1, 0)])
-    partial = project(core, attended, w_out, (), f32)
-    return project(1 - core, other, w_out, (partial,), bf16)
+    return project(core, attended, other, w_out)
 
 
 def solution(mesh):

time: 125 us -> 115 us (0.920)
  the two profiles are of different devices: /device:TPU:8 before, /device:TPU:89 now
where the time goes in v3:
time: 115 us; the launch traced here: 114 us
  starting transfers between devices  46.8 us (41%)
  blocking collectives  26.6 us (23%)
  Pallas kernels  23.8 us (21%)
  local copies, waits for them, and re-layouts  6.92 us (6%)
  waiting for transfers between devices  6.55 us (6%)
  other arithmetic  3.14 us (3%)
    ppermute x6, starting transfers between devices, along_row(): lax.ppermute(block, 'sp', [(i, i // ROW * ROW + (i + steps) % ROW) for i...  27.7 us
    all_to_all x1, blocking collectives, shards(): held = exchange(held)  26.6 us
    ppermute x2, starting transfers between devices, onward(): lax.ppermute(block, 'sp', [(i, i + distance) for i in range(devices - dis...  7.24 us
    all_to_all x1, starting transfers between devices, shards(): far = exchange(far)  6.47 us
    pallas_call x1, Pallas kernels, near_attention(): pl.pallas_call(near_kernel, in_specs=[pl.BlockSpec(memory_space=pltpu.SME...  5.67 us
    ppermute x6, waiting for transfers between devices, along_row(): lax.ppermute(block, 'sp', [(i, i // ROW * ROW + (i + steps) % ROW) for i...  4.99 us
    pallas_call x1, Pallas kernels, plane_pieces(): pl.pallas_call(plane_pieces_kernel, in_specs=[vmem, vmem, hbm, hbm, hbm],...  4.45 us
    unnamed x8, local copies, waits for them, and re-layouts  4.14 us
  transfers between devices with their start and end apart: 14, of which 3 were waited for; matrix products, arithmetic and copies ran while one was open for 3% of the time, Pallas kernels for 14%

profile of v3, /device:TPU:89, one launch (start us, length us, event | category | flops | bytes accessed | tf_op | source)
XLA Modules:
  0.0 113.9 jit_solution(3382255150396147346)
XLA Ops:
  0.0 1.2 %multiply_sine_fusion = (f32[256,64]{1,0:T(8,128)}, f32[256,64]{1,0:T(8,128)}) fusion(f32[64]{0:T(128)S(1)} %multiply_power_fusion, f32[256]{0:T(256)S(1)} %add_convert_fusion), kind=kLoop, calls=%fused_computation.1 | loop fusion | flops 16384 | bytes 132352 | tf_op jit(solution)/shard_map/sin | solution.py:396
  1.3 4.5 %plane_pieces.1 = bf16[16,3,128,128]{3,2,1,0:T(8,128)(2,1)} custom-call(f32[256,64]{1,0:T(8,128)} %get-tuple-element.34.cos_ref, f32[256,64]{1,0:T(8,128)} %get-tuple-element.33.sin_ref, bf16[3,256,1024]{2,1,0:T(8,128)(2,1)} %k_ref.3, bf16[3,256,1024]{2,1,0:T(8,128)(2,1)} %v_ref.3, bf16[3,256,1024]{2,1,0:T(8,128)(2,1)} %q_ref.3), custom_call_target="tpu_custom_call" | custom-call | flops 1073741824 | bytes 3145728 | tf_op jit(solution)/shard_map/plane_pieces/pallas_call | solution.py:78
  5.7 26.6 %all_to_all.10.in_ref = bf16[16,3,128,128]{3,2,1,0:T(8,128)(2,1)S(1)} all-to-all(bf16[16,3,128,128]{3,2,1,0:T(8,128)(2,1)} %plane_pieces.1), channel_id=1, replica_groups={{0,2,4,6,8,10,12,14,16,18,20,22,24,26,28,30},{32,34,36,38,40,42,44,46,4..., dimensions={0} | all-to-all | bytes 3145728 | tf_op jit(solution)/shard_map/all_to_all | solution.py:424
  32.3 0.8 slice.12
  33.1 3.5 %collective-permute-start.1 = (bf16[8,2,128,128]{3,2,1,0:T(8,128)(2,1)}, bf16[8,2,128,128]{3,2,1,0:T(8,128)(2,1)S(1)}, u32[]{:S(2)}, u32[]{:S(2)}) collective-permute-start(bf16[8,2,128,128]{3,2,1,0:T(8,128)(2,1)} %slice.12), channel_id=1, source_target_pairs={{0,32},{2,34},{4,36},{6,38},{8,40},{10,42},{12,44},{14,46},{16,48}... | collective-permute-start | bytes 1572872 | tf_op jit(solution)/shard_map/ppermute | solution.py:415
  36.7 3.9 %row_pieces.1 = (bf16[3,2,256,128]{3,2,1,0:T(8,128)(2,1)}, bf16[3,2,256,128]{3,2,1,0:T(8,128)(2,1)}, bf16[3,2,256,128]{3,2,1,0:T(8,128)(2,1)}, bf16[3,2,256,128]...) custom-call(s32[1]{0:T(128)} %bitcast.1.x_ref, ...), custom_call_target="tpu_custom_call" | custom-call | flops 1073741824 | bytes 3145728 | tf_op jit(solution)/shard_map/row_pieces/pallas_call | solution.py:126
  40.6 0.7 collective-permute-start.5
  41.2 0.3 collective-permute-start.2
  41.5 1.3 %collective-permute-start.6 = (bf16[2,2,256,128]{3,2,1,0:T(8,128)(2,1)}, bf16[2,2,256,128]{3,2,1,0:T(8,128)(2,1)}, u32[]{:S(2)}, u32[]{:S(2)}) collective-permute-start(bf16[2,2,256,128]{3,2,1,0:T(8,128)(2,1)} %get-tuple-element.26), channel_id=1, source_target_pairs={{4,14},{6,8},{12,22},{14,16},{20,30},{22,24},{28,38},{30,32},{36,4... | collective-permute-start | bytes 786440 | tf_op jit(solution)/shard_map/ppermute | solution.py:412
  42.8 1.3 %collective-permute-start.7 = (bf16[2,2,256,128]{3,2,1,0:T(8,128)(2,1)}, bf16[2,2,256,128]{3,2,1,0:T(8,128)(2,1)}, u32[]{:S(2)}, u32[]{:S(2)}) collective-permute-start(bf16[2,2,256,128]{3,2,1,0:T(8,128)(2,1)} %get-tuple-element.27), channel_id=1, source_target_pairs={{4,8},{6,10},{12,16},{14,18},{20,24},{22,26},{28,32},{30,34},{36,4... | collective-permute-start | bytes 786440 | tf_op jit(solution)/shard_map/ppermute | solution.py:412
  44.1 1.0 slice.10
  45.1 1.0 slice.9
  46.1 0.8 pad_maximum_fusion
  46.9 0.0 collective-permute-done.5.refs_4_
  46.9 9.7 %collective-permute-start.3 = (bf16[3,2,256,128]{3,2,1,0:T(8,128)(2,1)}, bf16[3,2,256,128]{3,2,1,0:T(8,128)(2,1)S(1)}, u32[]{:S(2)}, u32[]{:S(2)}) collective-permute-start(bf16[3,2,256,128]{3,2,1,0:T(8,128)(2,1)} %get-tuple-element.23), channel_id=1, source_target_pairs={{0,4},{2,6},{4,0},{6,2},{8,12},{10,14},{12,8},{14,10},{16,20},{18,... | collective-permute-start | bytes 1179656 | tf_op jit(solution)/shard_map/ppermute | solution.py:408
  56.7 0.0 collective-permute-done.1.halo_ref
  56.7 0.1 collective-permute-start.4
  56.7 0.0 copy-start.3
  56.7 2.5 %plane_attention.1 = bf16[16,144,128]{2,1,0:T(8,128)(2,1)} custom-call(s32[1]{0:T(128)} %bitcast.3.z_ref, bf16[16,3,128,128]{3,2,1,0:T(8,128)(2,1)S(1)} %all_to_all.10.in_ref, bf16[8,2,128,128]{3,2,1,0:T(8,128)(2,1)S(1)} %collective-permute-done.1.halo_ref), custom_call_target="tpu_custom_call" | custom-call | flops 2147483648 | bytes 3145728 | tf_op jit(solution)/shard_map/plane_attention/pallas_call | solution.py:209
  59.3 6.5 %all-to-all-start.1 = ((bf16[16,144,128]{2,1,0:T(8,128)(2,1)}), bf16[16,144,128]{2,1,0:T(8,128)(2,1)S(1)}, u32[]{:S(2)}, u32[]{:S(2)}) async-start(bf16[16,144,128]{2,1,0:T(8,128)(2,1)} %plane_attention.1), calls=%async_computation.1 | async-start | bytes 1179648 | tf_op jit(solution)/shard_map/all_to_all | solution.py:433
  65.7 0.0 collective-permute-done.6.refs_5_
  65.7 0.7 collective-permute-start.8
  66.4 0.0 collective-permute-done.7.refs_6_
  66.4 3.7 %collective-permute-start = (bf16[2,128,1024]{2,1,0:T(8,128)(2,1)}, bf16[2,128,1024]{2,1,0:T(8,128)(2,1)}, u32[]{:S(2)}, u32[]{:S(2)}) collective-permute-start(bf16[2,128,1024]{2,1,0:T(8,128)(2,1)} %pad_maximum_fusion), channel_id=1, source_target_pairs={{0,2},{2,4},{4,6},{6,8},{8,10},{10,12},{12,14},{14,16},{16,18},{18... | collective-permute-start | bytes 1572872 | tf_op jit(solution)/shard_map/ppermute | solution.py:415
  70.1 1.0 multiply_sine_fusion.1
  71.1 0.1 pad_add_fusion.x_ref
  71.2 0.0 collective-permute-done.8.refs_7_
  71.2 0.0 collective-permute-done.2.refs_1_
  71.2 4.2 %collective-permute-done.3.refs_2_ = bf16[3,2,256,128]{3,2,1,0:T(8,128)(2,1)S(1)} collective-permute-done((bf16[3,2,256,128]{3,2,1,0:T(8,128)(2,1)}, bf16[3,2,256,128]{3,2,1,0:T(8,128)(2,1)S(1)}, u32[]{:S(2)}, u32[]{:S(2)}) %collective-permute-start.3) | collective-permute-done | bytes 393248 | tf_op jit(solution)/shard_map/ppermute | solution.py:408
  75.4 0.0 collective-permute-done.4.refs_3_
  75.4 0.0 copy-done.3
  75.4 3.4 %row_attention.1 = (bf16[2,272,128]{2,1,0:T(8,128)(2,1)S(1)}, bf16[2,272,128]{2,1,0:T(8,128)(2,1)S(1)}, bf16[2,272,128]{2,1,0:T(8,128)(2,1)S(1)}, bf16[2,272,128]{2,1,0:T(8,128)(2,1)S(1)}) custom-call(s32[2]{0:T(128)S(1)} %pad_add_fusion.x_ref, bf16[3,2,256,128]{3,2,1,0:T(8,128)(2,1)S(1)} %copy-done.3, ...), custom_call_target="tpu_custom_call" | custom-call | flops 2147483648 | bytes 3145728 | tf_op jit(solution)/shard_map/row_attention/pallas_call | solution.py:260
  78.8 13.4 %collective-permute-start.10 = (bf16[2,272,128]{2,1,0:T(8,128)(2,1)S(1)}, bf16[2,272,128]{2,1,0:T(8,128)(2,1)S(1)}, u32[]{:S(2)}, u32[]{:S(2)}) collective-permute-start(bf16[2,272,128]{2,1,0:T(8,128)(2,1)S(1)} %get-tuple-element.31), channel_id=1, source_target_pairs={{0,4},{2,6},{4,0},{6,2},{8,12},{10,14},{12,8},{14,10},{16,20},{18,... | collective-permute-start | bytes 417800 | tf_op jit(solution)/shard_map/ppermute | solution.py:408
  92.2 4.3 %collective-permute-start.11 = (bf16[2,272,128]{2,1,0:T(8,128)(2,1)S(1)}, bf16[2,272,128]{2,1,0:T(8,128)(2,1)S(1)}, u32[]{:S(2)}, u32[]{:S(2)}) collective-permute-start(bf16[2,272,128]{2,1,0:T(8,128)(2,1)S(1)} %get-tuple-element.32), channel_id=1, source_target_pairs={{0,6},{2,0},{4,2},{6,4},{8,14},{10,8},{12,10},{14,12},{16,22},{18,... | collective-permute-start | bytes 417800 | tf_op jit(solution)/shard_map/ppermute | solution.py:408
  96.5 0.0 collective-permute-start.9
  96.5 0.0 collective-permute-done.halo_ref
  96.5 5.7 %near_attention.1 = (bf16[256,1024]{1,0:T(8,128)(2,1)}, f32[256,128]{1,0:T(8,128)}) custom-call(s32[1]{0:T(128)} %bitcast.2.z_ref, f32[256,64]{1,0:T(8,128)} %get-tuple-element.34.cos_ref, f32[256,64]{1,0:T(8,128)} %get-tuple-element.33.sin_ref, f32[128,64]{1,0:T(8,128)} %get-tuple-element.36.pcos_ref, f32[128,64]{1,0:T(8,128)} %get-tuple-element.35.psin_ref, ...), custom_call_target="tpu_custom_call" | custom-call | flops 2147483648 | bytes 4194304 | tf_op jit(solution)/shard_map/near_attention/pallas_call | solution.py:312
  102.2 0.0 collective-permute-done.10.two_ref
  102.2 0.0 collective-permute-done.11.three_ref
  102.2 0.8 collective-permute-done.9.one_ref
  103.0 0.0 all-to-all-done.1.far_ref
  103.0 0.0 copy-start.1
  103.0 1.0 copy-done.1
  104.0 0.0 copy-start.2
  104.0 0.9 copy-done.2
  104.9 1.8 %merge_groups.1.mine_ref = bf16[256,1024]{1,0:T(8,128)(2,1)S(1)} custom-call(s32[1]{0:T(128)} %bitcast.1.x_ref, bf16[256,1024]{1,0:T(8,128)(2,1)S(1)} %copy-done.1, f32[256,128]{1,0:T(8,128)S(1)} %copy-done.2, bf16[16,144,128]{2,1,0:T(8,128)(2,1)S(1)} %all-to-all-done.1.far_ref, bf16[2,272,128]{2,1,0:T(8,128)(2,1)S(1)} %get-tuple-element.29.own_ref, ...), custom_call_target="tpu_custom_call" | custom-call | flops 16777216 | bytes 2097152 | tf_op jit(solution)/shard_map/merge_groups/pallas_call | solution.py:358
  106.7 1.4 %collective-permute-start.12 = (bf16[256,1024]{1,0:T(8,128)(2,1)S(1)}, bf16[256,1024]{1,0:T(8,128)(2,1)S(1)}, u32[]{:S(2)}, u32[]{:S(2)}) collective-permute-start(bf16[256,1024]{1,0:T(8,128)(2,1)S(1)} %merge_groups.1.mine_ref), channel_id=1, source_target_pairs={{0,1},{1,0},{2,3},{3,2},{4,5},{5,4},{6,7},{7,6},{8,9},{9,8},{10,11... | collective-permute-start | bytes 1572872 | tf_op jit(solution)/shard_map/ppermute | solution.py:437
  108.2 1.5 %collective-permute-done.12.other_ref = bf16[256,1024]{1,0:T(8,128)(2,1)S(1)} collective-permute-done((bf16[256,1024]{1,0:T(8,128)(2,1)S(1)}, bf16[256,1024]{1,0:T(8,128)(2,1)S(1)}, u32[]{:S(2)}, u32[]{:S(2)}) %collective-permute-start.12) | collective-permute-done | bytes 524320 | tf_op jit(solution)/shard_map/ppermute | solution.py:437
  109.7 0.0 copy-start
  109.7 2.2 %copy-done = bf16[2048,1024]{1,0:T(8,128)(2,1)S(1)} copy-done((bf16[2048,1024]{1,0:T(8,128)(2,1)S(1)}, bf16[2048,1024]{1,0:T(8,128)(2,1)}, u32[]{:S(2)}) %copy-start) | copy-done | bytes 4194328
  111.9 2.0 %project.1 = bf16[256,1024]{1,0:T(8,128)(2,1)} custom-call(s32[1]{0:T(128)} %bitcast.core_ref, bf16[256,1024]{1,0:T(8,128)(2,1)S(1)} %merge_groups.1.mine_ref, bf16[256,1024]{1,0:T(8,128)(2,1)S(1)} %collective-permute-done.12.other_ref, bf16[2048,1024]{1,0:T(8,128)(2,1)S(1)} %copy-done), custom_call_target="tpu_custom_call" | custom-call | flops 1073741824 | bytes 4194304 | tf_op jit(solution)/shard_map/project/pallas_call | solution.py:382
  (3 shorter events, 0.0 us)
Async XLA Ops:
  33.1 23.5 %collective-permute-start.1 = (bf16[8,2,128,128]{3,2,1,0:T(8,128)(2,1)}, bf16[8,2,128,128]{3,2,1,0:T(8,128)(2,1)S(1)}, u32[]{:S(2)}, u32[]{:S(2)}) collective-permute-start(bf16[8,2,128,128]{3,2,1,0:T(8,128)(2,1)} %slice.12), channel_id=1, source_target_pairs={{0,32},{2,34},{4,36},{6,38},{8,40},{10,42},{12,44},{14,46},{16,48}... | collective-permute-start | bytes 1572872 | tf_op jit(solution)/shard_map/ppermute | solution.py:415
  40.6 6.4 %collective-permute-start.5 = (bf16[2,2,256,128]{3,2,1,0:T(8,128)(2,1)}, bf16[2,2,256,128]{3,2,1,0:T(8,128)(2,1)S(1)}, u32[]{:S(2)}, u32[]{:S(2)}) collective-permute-start(bf16[2,2,256,128]{3,2,1,0:T(8,128)(2,1)} %get-tuple-element.25), channel_id=1, source_target_pairs={{4,12},{6,14},{12,20},{14,22},{20,28},{22,30},{28,36},{30,38},{36,... | collective-permute-start | bytes 786440 | tf_op jit(solution)/shard_map/ppermute | solution.py:412
  41.2 30.0 %collective-permute-start.2 = (bf16[3,2,256,128]{3,2,1,0:T(8,128)(2,1)}, bf16[3,2,256,128]{3,2,1,0:T(8,128)(2,1)S(1)}, u32[]{:S(2)}, u32[]{:S(2)}) collective-permute-start(bf16[3,2,256,128]{3,2,1,0:T(8,128)(2,1)} %get-tuple-element.22), channel_id=1, source_target_pairs={{0,2},{2,4},{4,6},{6,0},{8,10},{10,12},{12,14},{14,8},{16,18},{18,... | collective-permute-start | bytes 1179656 | tf_op jit(solution)/shard_map/ppermute | solution.py:408
  41.5 24.2 %collective-permute-start.6 = (bf16[2,2,256,128]{3,2,1,0:T(8,128)(2,1)}, bf16[2,2,256,128]{3,2,1,0:T(8,128)(2,1)}, u32[]{:S(2)}, u32[]{:S(2)}) collective-permute-start(bf16[2,2,256,128]{3,2,1,0:T(8,128)(2,1)} %get-tuple-element.26), channel_id=1, source_target_pairs={{4,14},{6,8},{12,22},{14,16},{20,30},{22,24},{28,38},{30,32},{36,4... | collective-permute-start | bytes 786440 | tf_op jit(solution)/shard_map/ppermute | solution.py:412
  42.8 23.6 %collective-permute-start.7 = (bf16[2,2,256,128]{3,2,1,0:T(8,128)(2,1)}, bf16[2,2,256,128]{3,2,1,0:T(8,128)(2,1)}, u32[]{:S(2)}, u32[]{:S(2)}) collective-permute-start(bf16[2,2,256,128]{3,2,1,0:T(8,128)(2,1)} %get-tuple-element.27), channel_id=1, source_target_pairs={{4,8},{6,10},{12,16},{14,18},{20,24},{22,26},{28,32},{30,34},{36,4... | collective-permute-start | bytes 786440 | tf_op jit(solution)/shard_map/ppermute | solution.py:412
  46.9 28.5 %collective-permute-start.3 = (bf16[3,2,256,128]{3,2,1,0:T(8,128)(2,1)}, bf16[3,2,256,128]{3,2,1,0:T(8,128)(2,1)S(1)}, u32[]{:S(2)}, u32[]{:S(2)}) collective-permute-start(bf16[3,2,256,128]{3,2,1,0:T(8,128)(2,1)} %get-tuple-element.23), channel_id=1, source_target_pairs={{0,4},{2,6},{4,0},{6,2},{8,12},{10,14},{12,8},{14,10},{16,20},{18,... | collective-permute-start | bytes 1179656 | tf_op jit(solution)/shard_map/ppermute | solution.py:408
  56.7 18.7 %collective-permute-start.4 = (bf16[3,2,256,128]{3,2,1,0:T(8,128)(2,1)}, bf16[3,2,256,128]{3,2,1,0:T(8,128)(2,1)}, u32[]{:S(2)}, u32[]{:S(2)}) collective-permute-start(bf16[3,2,256,128]{3,2,1,0:T(8,128)(2,1)} %get-tuple-element.24), channel_id=1, source_target_pairs={{0,6},{2,0},{4,2},{6,4},{8,14},{10,8},{12,10},{14,12},{16,22},{18,... | collective-permute-start | bytes 1179656 | tf_op jit(solution)/shard_map/ppermute | solution.py:408
  56.7 18.7 %copy-start.3 = (bf16[3,2,256,128]{3,2,1,0:T(8,128)(2,1)S(1)}, bf16[3,2,256,128]{3,2,1,0:T(8,128)(2,1)}, u32[]{:S(2)}) copy-start(bf16[3,2,256,128]{3,2,1,0:T(8,128)(2,1)} %get-tuple-element.21.refs_0_) | copy-start | bytes 1179652
  59.3 43.7 %all-to-all-start.1 = ((bf16[16,144,128]{2,1,0:T(8,128)(2,1)}), bf16[16,144,128]{2,1,0:T(8,128)(2,1)S(1)}, u32[]{:S(2)}, u32[]{:S(2)}) async-start(bf16[16,144,128]{2,1,0:T(8,128)(2,1)} %plane_attention.1), calls=%async_computation.1 | async-start | bytes 1179648 | tf_op jit(solution)/shard_map/all_to_all | solution.py:433
  65.7 5.5 %collective-permute-start.8 = (bf16[2,2,256,128]{3,2,1,0:T(8,128)(2,1)}, bf16[2,2,256,128]{3,2,1,0:T(8,128)(2,1)S(1)}, u32[]{:S(2)}, u32[]{:S(2)}) collective-permute-start(bf16[2,2,256,128]{3,2,1,0:T(8,128)(2,1)} %get-tuple-element.28), channel_id=1, source_target_pairs={{4,10},{6,12},{12,18},{14,20},{20,26},{22,28},{28,34},{30,36},{36,... | collective-permute-start | bytes 786440 | tf_op jit(solution)/shard_map/ppermute | solution.py:412
  66.4 30.0 %collective-permute-start = (bf16[2,128,1024]{2,1,0:T(8,128)(2,1)}, bf16[2,128,1024]{2,1,0:T(8,128)(2,1)}, u32[]{:S(2)}, u32[]{:S(2)}) collective-permute-start(bf16[2,128,1024]{2,1,0:T(8,128)(2,1)} %pad_maximum_fusion), channel_id=1, source_target_pairs={{0,2},{2,4},{4,6},{6,8},{8,10},{10,12},{12,14},{14,16},{16,18},{18... | collective-permute-start | bytes 1572872 | tf_op jit(solution)/shard_map/ppermute | solution.py:415
  78.8 23.4 %collective-permute-start.10 = (bf16[2,272,128]{2,1,0:T(8,128)(2,1)S(1)}, bf16[2,272,128]{2,1,0:T(8,128)(2,1)S(1)}, u32[]{:S(2)}, u32[]{:S(2)}) collective-permute-start(bf16[2,272,128]{2,1,0:T(8,128)(2,1)S(1)} %get-tuple-element.31), channel_id=1, source_target_pairs={{0,4},{2,6},{4,0},{6,2},{8,12},{10,14},{12,8},{14,10},{16,20},{18,... | collective-permute-start | bytes 417800 | tf_op jit(solution)/shard_map/ppermute | solution.py:408
  92.2 10.0 %collective-permute-start.11 = (bf16[2,272,128]{2,1,0:T(8,128)(2,1)S(1)}, bf16[2,272,128]{2,1,0:T(8,128)(2,1)S(1)}, u32[]{:S(2)}, u32[]{:S(2)}) collective-permute-start(bf16[2,272,128]{2,1,0:T(8,128)(2,1)S(1)} %get-tuple-element.32), channel_id=1, source_target_pairs={{0,6},{2,0},{4,2},{6,4},{8,14},{10,8},{12,10},{14,12},{16,22},{18,... | collective-permute-start | bytes 417800 | tf_op jit(solution)/shard_map/ppermute | solution.py:408
  96.5 6.5 %collective-permute-start.9 = (bf16[2,272,128]{2,1,0:T(8,128)(2,1)S(1)}, bf16[2,272,128]{2,1,0:T(8,128)(2,1)S(1)}, u32[]{:S(2)}, u32[]{:S(2)}) collective-permute-start(bf16[2,272,128]{2,1,0:T(8,128)(2,1)S(1)} %get-tuple-element.30), channel_id=1, source_target_pairs={{0,2},{2,4},{4,6},{6,0},{8,10},{10,12},{12,14},{14,8},{16,18},{18,... | collective-permute-start | bytes 417800 | tf_op jit(solution)/shard_map/ppermute | solution.py:408
  103.0 1.0 copy-start.1
  104.0 0.9 copy-start.2
  106.7 3.0 %collective-permute-start.12 = (bf16[256,1024]{1,0:T(8,128)(2,1)S(1)}, bf16[256,1024]{1,0:T(8,128)(2,1)S(1)}, u32[]{:S(2)}, u32[]{:S(2)}) collective-permute-start(bf16[256,1024]{1,0:T(8,128)(2,1)S(1)} %merge_groups.1.mine_ref), channel_id=1, source_target_pairs={{0,1},{1,0},{2,3},{3,2},{4,5},{5,4},{6,7},{7,6},{8,9},{9,8},{10,11... | collective-permute-start | bytes 1572872 | tf_op jit(solution)/shard_map/ppermute | solution.py:437
  109.7 2.2 %copy-start = (bf16[2048,1024]{1,0:T(8,128)(2,1)S(1)}, bf16[2048,1024]{1,0:T(8,128)(2,1)}, u32[]{:S(2)}) copy-start(bf16[2048,1024]{1,0:T(8,128)(2,1)} %w_ref.1) | copy-start | bytes 12582916
